TPU v7x, 32 devices: a whole 2x2x4 slice. The times are simulated.
32 devices in a mesh: sp: 4 (over z), fs: 4 (over y, x), tp: 2 (over core).
Axes of the slice: x: 2, y: 2, z: 4, core: 2. Of those that a mesh axis runs over, the one named last changes fastest.
Arguments:
- tokens: bfloat16 [4, 512, 4096], P('fs', 'sp'), may hold values from -6 to 6
- norm_gain: float32 [4096], replicated, may hold values from 0.1 to 1.9
- pool_proj: bfloat16 [4096, 1024], P(('sp', 'fs'), 'tp'), may hold values from -0.09375 to 0.09375
- query_proj: bfloat16 [4096, 1024], P(('sp', 'fs'), 'tp'), may hold values from -0.09375 to 0.09375
- key_proj: bfloat16 [4096, 1024], P(('sp', 'fs'), 'tp'), may hold values from -0.09375 to 0.09375
- value_proj: bfloat16 [4096, 1024], P(('sp', 'fs'), 'tp'), may hold values from -0.09375 to 0.09375
- pool_map: bfloat16 [4, 256, 256], replicated, may hold values from -0.375 to 0.375
- pool_scale: float32 [1024], replicated, may hold values from 0.1 to 1.9
- decay_rate: float32 [4], P('tp'), may hold values from 2e-05 to 0.034
- start_state: float32 [4, 4, 256, 256], P('fs', 'tp', 'sp'), may hold values from -96 to 96
- pool_back: bfloat16 [1024, 4096], P('tp', ('sp', 'fs')), may hold values from -0.125 to 0.125
- retention_back: bfloat16 [1024, 4096], P('tp', ('sp', 'fs')), may hold values from -0.125 to 0.125
Outputs:
- mixed: bfloat16 [4, 512, 4096], P('fs', ('sp', 'tp'))
All inputs are finite; a program needn't handle non-finite values.
Results may differ from a plain program's by a relative error of at most 0.014.
Values may be sent and summed in bfloat16 or wider, within the bound.
A program may use at most 128 MiB of HBM per device.

v0:
```python
import functools

from jax.experimental import pallas as pl
from jax.experimental.pallas import tpu as pltpu

import jax
import jax.numpy as jnp
from jax import lax
from jax.sharding import PartitionSpec as P

GROUPS = 4
BLOCK = 128
HALO = 16


eps = 1e-06
rope_base = 10000.0
highest_precision = lax.Precision.HIGHEST
window_list = (2, 4, 8, 16)


def shortened(x):
    return jax.tree.map(lambda a: a.astype(jnp.bfloat16) if a.dtype == jnp.float32 else a, x)


def shifted(x, axis, by):
    devices = lax.axis_size(axis)
    pairs = [(i, i + by) for i in range(devices) if 0 <= i + by < devices]
    return lax.ppermute(x, axis, pairs)


def carried_in(value, axis, join, neutral):
    count, mine = (lax.axis_size(axis), lax.axis_index(axis))
    pieces = jax.tree.map(lambda part: lax.all_gather(part, axis), value)
    running = jax.tree.map(
        lambda part, zero: jnp.full_like(part, 0) + jnp.asarray(zero, part.dtype), value, neutral
    )

    def turn(position, running):
        longer = join(running, jax.tree.map(lambda part: part[position], pieces))
        return jax.tree.map(lambda new, old: jnp.where(position < mine, new, old), longer, running)

    return lax.fori_loop(0, count - 1, turn, running)


def rotate(values, positions):
    half_dim = values.shape[-1] // 2
    inv_freq = 1.0 / rope_base ** jnp.linspace(0.0, 1.0, half_dim, dtype=jnp.float32)
    angles = positions.astype(jnp.float32)[:, None] * inv_freq[None, :]
    cosine = jnp.cos(angles)[:, None, :]
    sine = jnp.sin(angles)[:, None, :]
    first_half = values[..., :half_dim]
    second_half = values[..., half_dim:]
    return jnp.concatenate(
        [first_half * cosine - second_half * sine, first_half * sine + second_half * cosine],
        axis=-1,
    )


def trailing_sums(extended, length):
    begin = extended.shape[0] - length
    running = extended[begin:]
    results = []
    for behind in range(1, 16):
        running = running + extended[begin - behind : begin - behind + length]
        if behind + 1 in window_list:
            results.append(running)
    return results


def reshape_blocks(array):
    return array.reshape((array.shape[0] // BLOCK, BLOCK) + array.shape[1:])


def block_retention(queries, keys_in, values_in, decay_rate, initial):
    length, head_count, head_dim = queries.shape
    within = jnp.arange(BLOCK, dtype=jnp.float32)
    distance = within[:, None] - within[None, :]
    decay_mask = jnp.where(
        distance[None] >= 0,
        jnp.exp(-jnp.maximum(distance, 0.0)[None] * decay_rate[:, None, None]),
        0.0,
    )
    query_decay_factor = jnp.exp(-(within + 1.0)[:, None] * decay_rate[None, :])
    key_decay_factor = jnp.exp(-(BLOCK - 1.0 - within)[:, None] * decay_rate[None, :])
    block_decay_factor = jnp.exp(-BLOCK * decay_rate)

    def advance(state_carry, inputs):
        block_queries, block_keys, block_values = inputs
        scores = (
            jnp.einsum("ihk,jhk->hij", block_queries, block_keys, precision=highest_precision)
            * decay_mask
        )
        inside = jnp.einsum("hij,jhv->ihv", scores, block_values, precision=highest_precision)
        across_blocks = jnp.einsum(
            "bzy,zyx->bzx",
            block_queries * query_decay_factor[:, :, None],
            state_carry,
            precision=highest_precision,
        )
        state_carry = state_carry * block_decay_factor[:, None, None] + jnp.einsum(
            "flm,fld->lmd",
            block_keys * key_decay_factor[:, :, None],
            block_values,
            precision=highest_precision,
        )
        return (state_carry, inside + across_blocks)

    final_state, outputs = lax.scan(
        advance,
        initial,
        (reshape_blocks(queries), reshape_blocks(keys_in), reshape_blocks(values_in)),
    )
    return (outputs.reshape(length, head_count, values_in.shape[-1]), final_state)


def combine_states(earlier, latter):
    return (earlier[0] * latter[0], latter[0][:, None, None] * earlier[1] + latter[1])


def on_device(
    tokens,
    norm_gain,
    pool_proj,
    query_proj,
    key_proj,
    value_proj,
    pool_map,
    pool_scale,
    decay_rate,
    start_state,
    pool_back,
    retention_back,
):
    sequence = tokens[0]
    length = sequence.shape[0]
    tp_index = lax.axis_index("tp")
    sp_index = lax.axis_index("sp")
    tp_count = lax.axis_size("tp")
    floats = sequence.astype(jnp.float32)
    normed = (
        floats * lax.rsqrt(jnp.mean(floats * floats, axis=-1, keepdims=True) + eps) * norm_gain
    ).astype(jnp.bfloat16)
    group_normed = lax.all_gather(normed, "fs", axis=0, tiled=True)
    quarters = (
        lax.all_to_all(pool_proj, "fs", split_axis=1, concat_axis=0, tiled=True),
        lax.all_to_all(query_proj, "fs", split_axis=1, concat_axis=0, tiled=True),
        lax.all_to_all(key_proj, "fs", split_axis=1, concat_axis=0, tiled=True),
        lax.all_to_all(value_proj, "fs", split_axis=1, concat_axis=0, tiled=True),
    )
    pieces = (
        lax.all_gather(quarters[0], "sp", axis=0, tiled=True),
        lax.all_gather(quarters[1], "sp", axis=0, tiled=True),
        lax.all_gather(quarters[2], "sp", axis=0, tiled=True),
        lax.all_gather(quarters[3], "sp", axis=0, tiled=True),
    )
    partial_cols = tuple(
        (jnp.dot(group_normed, piece_w, preferred_element_type=jnp.float32) for piece_w in pieces)
    )
    rounded = tuple((result.astype(jnp.bfloat16) for result in partial_cols))
    pool_in, query_bf, key_bf, value_bf = jax.tree.map(
        lambda part, own: part.astype(own.dtype),
        lax.all_to_all(shortened(rounded), "fs", split_axis=0, concat_axis=1, tiled=True),
        rounded,
    )
    positions = jnp.arange(length, dtype=jnp.int32) + sp_index * length
    before = shifted(pool_in[length - HALO :], "sp", 1)
    extended = jnp.concatenate([before, pool_in], axis=0).astype(jnp.float32)
    stacked = jnp.stack(trailing_sums(extended, length))
    local_groups = GROUPS // tp_count
    channels = pool_in.shape[1]
    group_dim = channels // local_groups
    group_maps = lax.dynamic_slice_in_dim(pool_map, tp_index * local_groups, local_groups, 0)
    scales = lax.dynamic_slice_in_dim(pool_scale, tp_index * channels, channels, 0)
    windows = jnp.array(window_list, dtype=jnp.int32)
    pieces = []
    for group_idx in range(local_groups):
        chosen_group = tp_index * local_groups + group_idx
        lower = group_idx * group_dim
        chosen = lax.dynamic_index_in_dim(stacked, chosen_group, 0, keepdims=False)[
            :, lower : lower + group_dim
        ]
        counts = jnp.minimum(windows[chosen_group], positions + 1).astype(jnp.float32)
        inputs = extended[HALO:, lower : lower + group_dim]
        differ = (chosen / counts[:, None] - inputs).astype(jnp.bfloat16)
        pieces.append(jnp.dot(differ, group_maps[group_idx], preferred_element_type=jnp.float32))
    pool_out = (jnp.concatenate(pieces, axis=1) * scales).astype(jnp.bfloat16)
    head_count = decay_rate.shape[0]
    head_dim = query_bf.shape[1] // head_count
    queries = rotate(query_bf.astype(jnp.float32).reshape(length, head_count, head_dim), positions)
    keys_in = rotate(
        key_bf.astype(jnp.float32).reshape(length, head_count, head_dim), positions
    ) * head_dim ** (-0.5)
    values_in = value_bf.astype(jnp.float32).reshape(length, head_count, head_dim)
    zeros_state = jnp.zeros((head_count, head_dim, head_dim), jnp.float32)
    local_output, local_state = block_retention(
        queries, keys_in, values_in, decay_rate, zeros_state
    )
    span_decay = jnp.exp(-decay_rate * length)
    whole_start = lax.all_gather(start_state, "sp", axis=2, tiled=True)[0]
    span_factor, carried_over = carried_in(
        (span_decay, local_state), "sp", combine_states, (jnp.ones_like(span_decay), zeros_state)
    )
    offset_float = (sp_index * length).astype(jnp.float32)
    carried_over = carried_over + jnp.exp(-decay_rate * offset_float)[:, None, None] * whole_start
    steps_in = jnp.arange(length, dtype=jnp.float32) + 1.0
    query_rows_scaled = queries * jnp.exp(-steps_in[:, None] * decay_rate[None, :])[:, :, None]
    retained_output = local_output + jnp.einsum(
        "lpi,pib->lpb", query_rows_scaled, carried_over, precision=highest_precision
    )
    retained_output = retained_output * lax.rsqrt(
        jnp.mean(retained_output * retained_output, axis=-1, keepdims=True) + eps
    )
    ret_out = retained_output.reshape(length, head_count * head_dim).astype(jnp.bfloat16)
    pool_cols, retention_cols = (
        lax.all_gather(pool_back, ("sp", "fs"), axis=1, tiled=True),
        lax.all_gather(retention_back, ("sp", "fs"), axis=1, tiled=True),
    )
    weight_local = jnp.concatenate([pool_cols, retention_cols], axis=0)
    joined = jnp.concatenate([pool_out, ret_out], axis=1)
    mixed = lax.psum_scatter(
        jnp.dot(joined, weight_local, preferred_element_type=jnp.float32).astype(jnp.bfloat16),
        "tp",
        scatter_dimension=0,
        tiled=True,
    )
    return mixed[None]


MESH = pl.DeviceIdType.MESH


def where_am_i():
    sp, fs, tp = (lax.axis_index(name) for name in ("sp", "fs", "tp"))
    return sp, fs, tp, fs // 2, fs % 2


def remote(src, dst, send, recv, target):
    return pltpu.make_async_remote_copy(
        src_ref=src, dst_ref=dst, send_sem=send, recv_sem=recv, device_id=target, device_id_type=MESH
    )


def greet(others):
    barrier = pltpu.get_barrier_semaphore()
    for other in others:
        pl.semaphore_signal(barrier, inc=1, device_id=other, device_id_type=MESH)
    pl.semaphore_wait(barrier, len(others))


def cols(index, size):
    return pl.ds(pl.multiple_of(index * size, size), size)


def project_kernel(
    tok, gain, wp, wq, wk, wv, state, pb, rb,
    joined, start, backs,
    xn, xg, wg, part, got,
    w_send, w_recv, w_local, x_send, x_recv, x_local, f_send, f_recv,
    s_send, s_recv, b_send, b_recv, b_local, p_send, p_recv, j_send, j_recv,
):
    sp, fs, tp, y, x = where_am_i()
    nsp, nfs = 4, 4
    span, width = tok.shape
    half = span // 2
    feats = width // nsp
    rows, group = wg.shape[2], wg.shape[3]
    mats = (wp, wq, wk, wv)
    partner = (sp, fs, 1 - tp)
    waits = []
    greet(
        [
            (lax.rem(sp + dz, nsp), 2 * lax.rem(y + dy, 2) + x, lax.rem(tp + dt, 2))
            for dz in range(nsp) for dy in range(2) for dt in range(2) if dz or dy or dt
        ]
        + [(sp, 2 * lax.rem(y + dy, 2) + 1 - x, tp) for dy in range(2)]
    )

    def send_mat(m):
        for d in (3, 1, 2):
            to = lax.rem(fs + d, nfs)
            c = remote(
                mats[m].at[:, cols(to // 2, group)], wg.at[m, fs], w_send.at[d - 1, m],
                w_recv.at[m, fs], (sp, to, tp),
            )
            c.start()
            waits.append(c)
        c = pltpu.make_async_copy(mats[m].at[:, cols(y, group)], wg.at[m, fs], w_local.at[m])
        c.start()
        return c

    own_w = [send_mat(0)]

    floats = tok[...].astype(jnp.float32)
    xn[...] = (
        floats * lax.rsqrt(jnp.mean(floats * floats, axis=-1, keepdims=True) + eps) * gain[...]
    ).astype(jnp.bfloat16)

    mine = pl.ds(pl.multiple_of(tp * half, half), half)

    def slot_of(from_y, from_sp):
        return xg.at[from_y, pl.ds(pl.multiple_of(from_sp * span + tp * half, half), half)]

    peer = (sp, 2 * (1 - y) + x, tp)
    for dz in (2, 1, 3, 0):
        to_sp = lax.rem(sp + dz, nsp)
        c = remote(
            xn.at[mine, cols(to_sp, feats)], slot_of(y, sp), x_send.at[dz], x_recv.at[y, sp],
            (to_sp, fs, tp) if dz else peer,
        )
        c.start()
        waits.append(c)
    own_x = pltpu.make_async_copy(
        xn.at[:, cols(sp, feats)], xg.at[y, pl.ds(pl.multiple_of(sp * span, span), span)], x_local
    )
    own_x.start()
    forwards = []

    def arrived(from_y, from_sp, order):
        slot = slot_of(from_y, from_sp)
        remote(slot, slot, x_send.at[0], x_recv.at[from_y, from_sp], partner).wait_recv()
        c = remote(slot, slot, f_send.at[order], f_recv.at[order], partner)
        c.start()
        forwards.append(c)
        return slot

    for dz in (1, 3, 2):
        fr_sp = lax.rem(sp + nsp - dz, nsp)
        slot = arrived(y, fr_sp, dz - 1)
        c = remote(slot, slot, x_send.at[nsp + dz - 1], x_recv.at[y, fr_sp], peer)
        c.start()
        waits.append(c)
    for m in range(1, 4):
        own_w.append(send_mat(m))
    for j in range(2):
        for h in range(2):
            to_sp, to_fs = 2 * y + tp, 2 * j + x
            rs = state.shape[1]
            dst = start.at[pl.ds(pl.multiple_of(sp * rs, rs), rs)]
            same = (to_sp == sp) & (to_fs == fs) & (tp == h)

            @pl.when(same)
            def _():
                pltpu.make_async_copy(state.at[j], dst, s_recv.at[sp]).start()

            @pl.when(jnp.logical_not(same))
            def _():
                remote(state.at[j], dst, s_send.at[2 * j + h], s_recv.at[sp], (to_sp, to_fs, h)).start()

    own_b = []
    for b, back in enumerate((pb, rb)):
        c = pltpu.make_async_copy(back, backs.at[fs, b], b_local.at[b])
        c.start()
        own_b.append(c)
        for d in (3, 1, 2):
            to = lax.rem(fs + d, nfs)
            c = remote(back, backs.at[fs, b], b_send.at[d - 1, b], b_recv.at[fs, b], (sp, to, tp))
            c.start()
            waits.append(c)

    own_x.wait()
    for c in forwards:
        c.wait()
    early = len(forwards)

    tall = 2 * span
    for m in range(4):
        own_w[m].wait()
        for d in range(1, nfs):
            fr = lax.rem(fs + nfs - d, nfs)
            remote(
                mats[m].at[:, cols(y, group)], wg.at[m, fr], w_send.at[d - 1, m], w_recv.at[m, fr], partner
            ).wait_recv()
        for s in (y, 1 - y):
            if m == 0 and s is not y:
                for dz in (0, 1, 3, 2):
                    arrived(1 - y, lax.rem(sp + nsp - dz, nsp), 3 + dz)
                for c in forwards[early:]:
                    c.wait()
            acc = jnp.zeros((2 * tall, group), jnp.float32)
            for f in range(nfs):
                acc += jnp.dot(
                    xg[s, :, f * rows : (f + 1) * rows], wg[m, f], preferred_element_type=jnp.float32
                )
            part[m, s] = acc.astype(jnp.bfloat16)
            for h in range(2):
                same = (2 * s + tp == sp) & (tp == h)
                src = part.at[m, s, h * tall : (h + 1) * tall]

                @pl.when(same)
                def _():
                    pltpu.make_async_copy(src, got.at[m, sp], p_recv.at[m, sp]).start()

                @pl.when(jnp.logical_not(same))
                def _():
                    remote(
                        src, got.at[m, sp], p_send.at[m, 2 * s + h], p_recv.at[m, sp], (2 * s + tp, fs, h)
                    ).start()

    here = pl.ds(pl.multiple_of(tp * tall, tall), tall)
    there = pl.ds(pl.multiple_of((1 - tp) * tall, tall), tall)
    lasts = []
    for m in range(4):
        for k in range(nsp):
            remote(got.at[m, k], got.at[m, k], p_send.at[0, 0], p_recv.at[m, k], partner).wait_recv()
        total = got[m, 0].astype(jnp.float32)
        for k in range(1, nsp):
            total += got[m, k].astype(jnp.float32)
        joined[m, here] = total.astype(jnp.bfloat16)
        c = remote(joined.at[m, here], joined.at[m, here], j_send.at[m], j_recv.at[m], partner)
        c.start()
        lasts.append(c)
    for m in range(4):
        lasts[m].wait_send()
        remote(joined.at[m, there], joined.at[m, there], j_send.at[m], j_recv.at[m], partner).wait_recv()

    for j in range(2):
        for h in range(2):
            to_sp, to_fs = 2 * y + tp, 2 * j + x
            same = (to_sp == sp) & (to_fs == fs) & (tp == h)

            @pl.when(jnp.logical_not(same))
            def _():
                remote(state.at[j], start.at[pl.ds(0, state.shape[1])], s_send.at[2 * j + h], s_recv.at[0], partner).wait_send()

            same_p = (2 * j + tp == sp) & (tp == h)

            @pl.when(jnp.logical_not(same_p))
            def _():
                for m in range(4):
                    remote(got.at[m, 0], got.at[m, 0], p_send.at[m, 2 * j + h], p_recv.at[m, 0], partner).wait_send()

    for k in range(nsp):
        rs = state.shape[1]
        slot = start.at[k * rs : (k + 1) * rs]
        remote(slot, slot, s_send.at[0], s_recv.at[k], partner).wait_recv()
    for b, back in enumerate((pb, rb)):
        own_b[b].wait()
        for d in range(1, nfs):
            fr = lax.rem(fs + nfs - d, nfs)
            remote(back, backs.at[fr, b], b_send.at[d - 1, b], b_recv.at[fr, b], partner).wait_recv()
    for c in waits:
        c.wait_send()


def output_kernel(
    yh, backs, out,
    yg, stage, accs, give, take, done,
    y_send, y_recv, t_send, t_recv, g_send, g_recv, o_send, o_recv,
):
    sp, fs, tp, y, x = where_am_i()
    nsp, nfs = 4, 4
    half, wide = yh.shape
    group = wide // 2
    block = backs.shape[3]
    few = out.shape[0]
    across = nfs * block
    partner = (sp, fs, 1 - tp)
    s, p = sp // 2, sp % 2
    peer = (sp, 2 * (1 - y) + x, tp)
    greet(
        [
            (lax.rem(sp + dz, nsp), fs, lax.rem(tp + dt, 2))
            for dz in range(nsp) for dt in range(2) if dz or dt
        ]
        + [peer]
    )
    few2 = half // 2
    for c in range(2):
        part = yh.at[c * few2 : (c + 1) * few2]
        for dz in (2, 1, 3, 0):
            k = lax.rem(sp + dz, nsp)
            for staged, dst, sem in (
                (False, yg.at[y, tp, c], y_recv.at[y, tp, c]), (True, stage.at[tp, c], t_recv.at[tp, c])
            ):
                kind = (s != y) if staged else (s == y)
                if dz:

                    @pl.when(kind)
                    def _():
                        remote(part, dst, y_send.at[dz, c], sem, (k, fs, p)).start()
                else:

                    @pl.when(kind & (p == tp))
                    def _():
                        pltpu.make_async_copy(part, dst, sem).start()

                    @pl.when(kind & (p != tp))
                    def _():
                        remote(part, dst, y_send.at[dz, c], sem, partner).start()

    passed = []

    def forward(c):
        for h in range(2):
            slot = stage.at[h, c]
            remote(slot, slot, y_send.at[0, 0], t_recv.at[h, c], partner).wait_recv()
            move = remote(slot, yg.at[y, h, c], t_send.at[h, c], y_recv.at[y, h, c], peer)
            move.start()
            passed.append(move)

    def multiply(c):
        gives = []
        for h in range(2):
            for q in range(2):
                slot = yg.at[q, h, c]
                remote(slot, slot, y_send.at[0, 0], y_recv.at[q, h, c], partner).wait_recv()
            k = 2 * h + c
            for f in range(nfs):
                acc = jnp.zeros((few2, block), jnp.float32)
                for q in range(2):
                    for b in range(2):
                        acc += jnp.dot(
                            yg[q, h, c, :, b * group : (b + 1) * group],
                            backs[f, b, q * group : (q + 1) * group, :],
                            preferred_element_type=jnp.float32,
                        )
                accs[k, :, f * block : (f + 1) * block] = acc
            give[k] = accs[k, pl.ds(pl.multiple_of((1 - tp) * few, few), few), :].astype(jnp.bfloat16)
            move = remote(give.at[k], take.at[k], g_send.at[k], g_recv.at[k], partner)
            move.start()
            gives.append(move)
        return gives

    def finish(c, gives):
        for h in range(2):
            k = 2 * h + c
            gives[h].wait()
            own = accs[k, pl.ds(pl.multiple_of(tp * few, few), few), :]
            done[k] = (own + take[k].astype(jnp.float32)).astype(jnp.bfloat16)
            dst = out.at[:, cols(sp, across)]

            @pl.when(sp == k)
            def _():
                pltpu.make_async_copy(done.at[k], dst, o_recv.at[sp]).start()

            @pl.when(sp != k)
            def _():
                remote(done.at[k], dst, o_send.at[k], o_recv.at[sp], (k, fs, tp)).start()

    forward(0)
    first = multiply(0)
    finish(0, first)
    forward(1)
    second = multiply(1)
    finish(1, second)

    for k in range(nsp):
        view = out.at[:, k * across : (k + 1) * across]
        remote(done.at[k], view, o_send.at[k], o_recv.at[k], partner).wait_recv()

        @pl.when(sp != k)
        def _():
            remote(done.at[k], view, o_send.at[k], o_recv.at[k], partner).wait_send()

    for c in range(2):
        slot = yg.at[0, 0, c]
        for dz in range(1, nsp):
            remote(slot, slot, y_send.at[dz, c], y_recv.at[0, 0, c], partner).wait_send()

        @pl.when(p != tp)
        def _():
            remote(slot, slot, y_send.at[0, c], y_recv.at[0, 0, c], partner).wait_send()

    for move in passed:
        move.wait_send()


def turned(values, cosine, sine):
    half_dim = values.shape[-1] // 2
    a, b = values[:, :half_dim], values[:, half_dim:]
    return jnp.concatenate([a * cosine - b * sine, a * sine + b * cosine], axis=-1)


def angles_of(positions, half_dim):
    inv_freq = 1.0 / rope_base ** jnp.linspace(0.0, 1.0, half_dim, dtype=jnp.float32)
    angles = positions.astype(jnp.float32)[:, None] * inv_freq[None, :]
    return jnp.cos(angles), jnp.sin(angles)


def paired(
    tokens, norm_gain, pool_proj, query_proj, key_proj, value_proj, pool_map, pool_scale,
    decay_rate, start_state, pool_back, retention_back,
):
    bf, f32 = jnp.bfloat16, jnp.float32
    sp, fs, tp, y, x = where_am_i()
    nsp = lax.axis_size("sp")
    tok = tokens[0]
    span, width = tok.shape
    rows, two = pool_proj.shape
    group = two // 2
    length = nsp * span
    half = length // 2
    vm, hbm = pl.BlockSpec(memory_space=pltpu.VMEM), pl.BlockSpec(memory_space=pl.ANY)
    dma = pltpu.SemaphoreType.DMA
    rs = start_state.shape[2]
    joined, start, backs = pl.pallas_call(
        project_kernel,
        out_shape=(
            jax.ShapeDtypeStruct((4, length, group), bf),
            jax.ShapeDtypeStruct((nsp * rs, group), bf),
            jax.ShapeDtypeStruct((4, 2) + pool_back.shape, bf),
        ),
        in_specs=[vm, vm, hbm, hbm, hbm, hbm, hbm, hbm, hbm],
        out_specs=(vm, vm, vm),
        scratch_shapes=[
            pltpu.VMEM((span, width), bf),
            pltpu.VMEM((2, nsp * span, width // nsp), bf),
            pltpu.VMEM((4, 4, rows, group), bf),
            pltpu.VMEM((4, 2, length, group), bf),
            pltpu.VMEM((4, nsp, half, group), bf),
            dma((3, 4)), dma((4, 4)), dma((4,)), dma((7,)), dma((2, nsp)), dma,
            dma((7,)), dma((7,)), dma((4,)), dma((nsp,)), dma((3, 2)), dma((4, 2)), dma((2,)),
            dma((4, 4)), dma((4, nsp)), dma((4,)), dma((4,)),
        ],
        compiler_params=pltpu.CompilerParams(collective_id=0, has_side_effects=True, vmem_limit_bytes=60 * 2**20),
        name="project",
    )(
        tok, norm_gain[None, :], pool_proj, query_proj, key_proj, value_proj,
        start_state[0].astype(bf), pool_back, retention_back,
    )
    mine = lax.dynamic_slice_in_dim(joined[1], tp * half, half, 0)
    head = 2 * (sp % 2) + y
    local = lax.dynamic_index_in_dim(decay_rate, y, 0, keepdims=False)
    other = lax.ppermute(decay_rate, "tp", [(0, 1), (1, 0)])
    rate = jnp.where(sp % 2 == tp, local, lax.dynamic_index_in_dim(other, y, 0, keepdims=False))
    every = jnp.arange(length, dtype=jnp.int32)
    position = tp * half + jnp.arange(half, dtype=jnp.int32)

    pool_all = jnp.concatenate([jnp.zeros((HALO, group), f32), joined[0].astype(f32)], axis=0)
    extended = lax.dynamic_slice_in_dim(pool_all, tp * half, half + HALO, 0)
    sums = trailing_sums(extended, half)
    windows = jnp.array(window_list, dtype=jnp.int32)
    chosen = sums[0]
    for i in range(1, GROUPS):
        chosen = jnp.where(head == i, sums[i], chosen)
    counts = jnp.minimum(windows[head], position + 1).astype(f32)
    differ = (chosen / counts[:, None] - extended[HALO:]).astype(bf)
    this_map = lax.dynamic_index_in_dim(pool_map, head, 0, keepdims=False)
    scale = lax.dynamic_slice_in_dim(pool_scale, head * group, group, 0)
    pool_out = (jnp.dot(differ, this_map, preferred_element_type=f32) * scale).astype(bf)

    cosine, sine = angles_of(every, group // 2)
    my_cos = lax.dynamic_slice_in_dim(cosine, tp * half, half, 0)
    my_sin = lax.dynamic_slice_in_dim(sine, tp * half, half, 0)
    rq = turned(mine.astype(f32), my_cos, my_sin)
    rk = turned(joined[2].astype(f32), cosine, sine) * group ** (-0.5)
    value = joined[3].astype(f32)
    gap = (position[:, None] - every[None, :]).astype(f32)
    mask = jnp.where(gap >= 0, jnp.exp(-jnp.maximum(gap, 0.0) * rate), 0.0)
    high = lax.Precision.HIGHEST
    scores = jnp.dot(rq, rk.T, precision=high) * mask
    fade = jnp.exp(-(position.astype(f32) + 1.0) * rate)
    ret = jnp.dot(scores, value, precision=high) + jnp.dot(
        rq * fade[:, None], start.astype(f32), precision=high
    )
    ret = ret * lax.rsqrt(jnp.mean(ret * ret, axis=-1, keepdims=True) + eps)
    yh = jnp.concatenate([pool_out, ret.astype(bf)], axis=1)

    few = span // 2
    return pl.pallas_call(
        output_kernel,
        out_shape=jax.ShapeDtypeStruct((few, width), bf),
        in_specs=[vm, vm],
        out_specs=vm,
        scratch_shapes=[
            pltpu.VMEM((2, 2, 2, span, 2 * group), bf),
            pltpu.VMEM((2, 2, span, 2 * group), bf),
            pltpu.VMEM((nsp, span, 4 * pool_back.shape[1]), f32),
            pltpu.VMEM((nsp, few, 4 * pool_back.shape[1]), bf),
            pltpu.VMEM((nsp, few, 4 * pool_back.shape[1]), bf),
            pltpu.VMEM((nsp, few, 4 * pool_back.shape[1]), bf),
            dma((nsp, 2)), dma((2, 2, 2)), dma((2, 2)), dma((2, 2)), dma((nsp,)), dma((nsp,)), dma((nsp,)), dma((nsp,)),
        ],
        compiler_params=pltpu.CompilerParams(collective_id=1, has_side_effects=True, vmem_limit_bytes=60 * 2**20),
        name="output",
    )(yh, backs)[None]


def solution(mesh):
    sizes = mesh.shape
    small = sizes["sp"] == 4 and sizes["fs"] == 4 and sizes["tp"] == 2
    placed = (
        P("fs", "sp", None),
        P(),
        P(("sp", "fs"), "tp"),
        P(("sp", "fs"), "tp"),
        P(("sp", "fs"), "tp"),
        P(("sp", "fs"), "tp"),
        P(),
        P(),
        P("tp"),
        P("fs", "tp", "sp", None),
        P("tp", ("sp", "fs")),
        P("tp", ("sp", "fs")),
    )
    return jax.shard_map(
        paired if small else on_device,
        mesh=mesh,
        in_specs=placed,
        out_specs=P("fs", ("sp", "tp"), None),
        check_vma=False,
    )
```

profile of v0, /device:TPU:29, one launch (start us, length us, event | category | flops | bytes accessed | tf_op | source)
XLA Modules:
  0.0 144.0 jit_solution(14646438877943453576)
XLA Ops:
  0.0 0.0 copy-start
  0.0 0.7 collective-permute-start
  0.7 1.3 dynamic_slice.36
  2.0 1.2 dynamic_slice.30
  3.2 0.7 minimum_convert_fusion
  3.9 1.5 %convert_bitcast_fusion.state = bf16[2,64,256]{2,1,0:T(8,128)(2,1)} fusion(f32[1,2,64,256]{3,2,1,0:T(8,128)} %param.22), kind=kLoop, calls=%fused_computation.50 | loop fusion | flops 32768 | bytes 196608 | tf_op jit(solution)/shard_map/convert_element_type | solution.py:620
  5.4 71.2 %project.1 = (bf16[4,512,256]{2,1,0:T(8,128)(2,1)}, bf16[256,256]{1,0:T(8,128)(2,1)}, bf16[4,2,512,256]{3,2,1,0:T(8,128)(2,1)}) custom-call(bf16[128,4096]{1,0:T(8,128)(2,1)} %bitcast.25, f32[1,4096]{1,0:T(1,128)} %bitcast.26, bf16[256,512]{1,0:T(8,128)(2,1)} %wp.1, bf16[256,512]{1,0:T(8,128)(2,1)} %wq.1, bf16[256,512]{1,0:T(8,128)(2,1)} %wk.1, ...), custom_call_target="tpu_custom_call" | custom-call | tf_op jit(solution)/shard_map/project/pallas_call | solution.py:597
  76.7 1.2 slice_bitcast_fusion
  77.9 0.8 dynamic_slice.32
  78.7 0.1 fusion.18
  78.8 1.2 multiply_cosine_fusion
  80.0 0.0 copy-done
  80.0 0.5 fusion
  80.6 0.0 copy-start.1
  80.6 0.0 collective-permute-done
  80.6 0.6 dynamic_slice.37
  82.4 0.7 convolution_multiply_fusion
  83.2 1.3 fusion.6
  84.5 0.0 copy-done.1
  84.5 0.4 multiply_reduce_fusion
  85.0 0.1 multiply_convert_fusion
  85.1 0.7 pad_maximum_fusion.1.yh
  85.8 56.3 %output.1 = bf16[64,4096]{1,0:T(8,128)(2,1)} custom-call(bf16[256,512]{1,0:T(8,128)(2,1)} %pad_maximum_fusion.1.yh, bf16[4,2,512,256]{3,2,1,0:T(8,128)(2,1)} %get-tuple-element.10.backs), custom_call_target="tpu_custom_call" | custom-call | tf_op jit(solution)/shard_map/output/pallas_call | solution.py:661
  142.1 1.9 %copy.21 = bf16[1,64,4096]{2,1,0:T(8,128)(2,1)} copy(bf16[1,64,4096]{2,1,0:T(8,128)(2,1)} %bitcast.24) | data formatting | bytes 1048576
  (7 shorter events, 0.1 us)
Async XLA Ops:
  0.0 80.0 %copy-start = (bf16[4,256,256]{2,1,0:T(8,128)(2,1)S(1)}, bf16[4,256,256]{2,1,0:T(8,128)(2,1)}, u32[]{:S(2)}) copy-start(bf16[4,256,256]{2,1,0:T(8,128)(2,1)} %param.19) | copy-start | bytes 1572868
  0.0 80.6 %collective-permute-start = (f32[2]{0:T(128)}, f32[2]{0:T(128)S(1)}, u32[]{:S(2)}, u32[]{:S(2)}) collective-permute-start(f32[2]{0:T(128)} %param.21), channel_id=1, source_target_pairs={{0,1},{1,0},{2,3},{3,2},{4,5},{5,4},{6,7},{7,6},{8,9},{9,8},{10,11... | collective-permute-start | bytes 32 | tf_op jit(solution)/shard_map/ppermute | solution.py:625
  80.6 4.0 %copy-start.1 = (bf16[256,256]{1,0:T(8,128)(2,1)S(1)}, bf16[256,256]{1,0:T(8,128)(2,1)}, u32[]{:S(2)}) copy-start(bf16[256,256]{1,0:T(8,128)(2,1)} %get-tuple-element.9) | copy-start | bytes 393220
where the time goes:
time: 146 us; the launch traced here: 144 us
  Pallas kernels  128 us (88%)
  local copies, waits for them, and re-layouts  5.76 us (4%)
  other arithmetic  5.58 us (4%)
  matrix products  3.01 us (2%)
    pallas_call x1, Pallas kernels, paired(): pl.pallas_call(project_kernel, out_shape=(jax.ShapeDtypeStruct((4, length...  71.2 us
    pallas_call x1, Pallas kernels, paired(): pl.pallas_call(output_kernel, out_shape=jax.ShapeDtypeStruct((few, width)...  56.3 us
  transfers between devices with their start and end apart: 1, of which 0 were waited for; matrix products, arithmetic and copies ran while one was open for 6% of the time, Pallas kernels for 49%

commit v1 on v0

v1 whole, which is shorter than its diff:
```python
import numpy as np
from jax.experimental import pallas as pl
from jax.experimental.pallas import tpu as pltpu

import jax
import jax.numpy as jnp
from jax import lax
from jax.sharding import PartitionSpec as P

GROUPS = 4
BLOCK = 128
HALO = 16


eps = 1e-06
rope_base = 10000.0
highest_precision = lax.Precision.HIGHEST
window_list = (2, 4, 8, 16)


def shortened(x):
    return jax.tree.map(lambda a: a.astype(jnp.bfloat16) if a.dtype == jnp.float32 else a, x)


def shifted(x, axis, by):
    devices = lax.axis_size(axis)
    pairs = [(i, i + by) for i in range(devices) if 0 <= i + by < devices]
    return lax.ppermute(x, axis, pairs)


def carried_in(value, axis, join, neutral):
    count, mine = (lax.axis_size(axis), lax.axis_index(axis))
    pieces = jax.tree.map(lambda part: lax.all_gather(part, axis), value)
    running = jax.tree.map(
        lambda part, zero: jnp.full_like(part, 0) + jnp.asarray(zero, part.dtype), value, neutral
    )

    def turn(position, running):
        longer = join(running, jax.tree.map(lambda part: part[position], pieces))
        return jax.tree.map(lambda new, old: jnp.where(position < mine, new, old), longer, running)

    return lax.fori_loop(0, count - 1, turn, running)


def rotate(values, positions):
    half_dim = values.shape[-1] // 2
    inv_freq = 1.0 / rope_base ** jnp.linspace(0.0, 1.0, half_dim, dtype=jnp.float32)
    angles = positions.astype(jnp.float32)[:, None] * inv_freq[None, :]
    cosine = jnp.cos(angles)[:, None, :]
    sine = jnp.sin(angles)[:, None, :]
    first_half = values[..., :half_dim]
    second_half = values[..., half_dim:]
    return jnp.concatenate(
        [first_half * cosine - second_half * sine, first_half * sine + second_half * cosine],
        axis=-1,
    )


def trailing_sums(extended, length):
    begin = extended.shape[0] - length
    running = extended[begin:]
    results = []
    for behind in range(1, 16):
        running = running + extended[begin - behind : begin - behind + length]
        if behind + 1 in window_list:
            results.append(running)
    return results


def reshape_blocks(array):
    return array.reshape((array.shape[0] // BLOCK, BLOCK) + array.shape[1:])


def block_retention(queries, keys_in, values_in, decay_rate, initial):
    length, head_count, head_dim = queries.shape
    within = jnp.arange(BLOCK, dtype=jnp.float32)
    distance = within[:, None] - within[None, :]
    decay_mask = jnp.where(
        distance[None] >= 0,
        jnp.exp(-jnp.maximum(distance, 0.0)[None] * decay_rate[:, None, None]),
        0.0,
    )
    query_decay_factor = jnp.exp(-(within + 1.0)[:, None] * decay_rate[None, :])
    key_decay_factor = jnp.exp(-(BLOCK - 1.0 - within)[:, None] * decay_rate[None, :])
    block_decay_factor = jnp.exp(-BLOCK * decay_rate)

    def advance(state_carry, inputs):
        block_queries, block_keys, block_values = inputs
        scores = (
            jnp.einsum("ihk,jhk->hij", block_queries, block_keys, precision=highest_precision)
            * decay_mask
        )
        inside = jnp.einsum("hij,jhv->ihv", scores, block_values, precision=highest_precision)
        across_blocks = jnp.einsum(
            "bzy,zyx->bzx",
            block_queries * query_decay_factor[:, :, None],
            state_carry,
            precision=highest_precision,
        )
        state_carry = state_carry * block_decay_factor[:, None, None] + jnp.einsum(
            "flm,fld->lmd",
            block_keys * key_decay_factor[:, :, None],
            block_values,
            precision=highest_precision,
        )
        return (state_carry, inside + across_blocks)

    final_state, outputs = lax.scan(
        advance,
        initial,
        (reshape_blocks(queries), reshape_blocks(keys_in), reshape_blocks(values_in)),
    )
    return (outputs.reshape(length, head_count, values_in.shape[-1]), final_state)


def combine_states(earlier, latter):
    return (earlier[0] * latter[0], latter[0][:, None, None] * earlier[1] + latter[1])


def on_device(
    tokens,
    norm_gain,
    pool_proj,
    query_proj,
    key_proj,
    value_proj,
    pool_map,
    pool_scale,
    decay_rate,
    start_state,
    pool_back,
    retention_back,
):
    sequence = tokens[0]
    length = sequence.shape[0]
    tp_index = lax.axis_index("tp")
    sp_index = lax.axis_index("sp")
    tp_count = lax.axis_size("tp")
    floats = sequence.astype(jnp.float32)
    normed = (
        floats * lax.rsqrt(jnp.mean(floats * floats, axis=-1, keepdims=True) + eps) * norm_gain
    ).astype(jnp.bfloat16)
    group_normed = lax.all_gather(normed, "fs", axis=0, tiled=True)
    quarters = (
        lax.all_to_all(pool_proj, "fs", split_axis=1, concat_axis=0, tiled=True),
        lax.all_to_all(query_proj, "fs", split_axis=1, concat_axis=0, tiled=True),
        lax.all_to_all(key_proj, "fs", split_axis=1, concat_axis=0, tiled=True),
        lax.all_to_all(value_proj, "fs", split_axis=1, concat_axis=0, tiled=True),
    )
    pieces = (
        lax.all_gather(quarters[0], "sp", axis=0, tiled=True),
        lax.all_gather(quarters[1], "sp", axis=0, tiled=True),
        lax.all_gather(quarters[2], "sp", axis=0, tiled=True),
        lax.all_gather(quarters[3], "sp", axis=0, tiled=True),
    )
    partial_cols = tuple(
        (jnp.dot(group_normed, piece_w, preferred_element_type=jnp.float32) for piece_w in pieces)
    )
    rounded = tuple((result.astype(jnp.bfloat16) for result in partial_cols))
    pool_in, query_bf, key_bf, value_bf = jax.tree.map(
        lambda part, own: part.astype(own.dtype),
        lax.all_to_all(shortened(rounded), "fs", split_axis=0, concat_axis=1, tiled=True),
        rounded,
    )
    positions = jnp.arange(length, dtype=jnp.int32) + sp_index * length
    before = shifted(pool_in[length - HALO :], "sp", 1)
    extended = jnp.concatenate([before, pool_in], axis=0).astype(jnp.float32)
    stacked = jnp.stack(trailing_sums(extended, length))
    local_groups = GROUPS // tp_count
    channels = pool_in.shape[1]
    group_dim = channels // local_groups
    group_maps = lax.dynamic_slice_in_dim(pool_map, tp_index * local_groups, local_groups, 0)
    scales = lax.dynamic_slice_in_dim(pool_scale, tp_index * channels, channels, 0)
    windows = jnp.array(window_list, dtype=jnp.int32)
    pieces = []
    for group_idx in range(local_groups):
        chosen_group = tp_index * local_groups + group_idx
        lower = group_idx * group_dim
        chosen = lax.dynamic_index_in_dim(stacked, chosen_group, 0, keepdims=False)[
            :, lower : lower + group_dim
        ]
        counts = jnp.minimum(windows[chosen_group], positions + 1).astype(jnp.float32)
        inputs = extended[HALO:, lower : lower + group_dim]
        differ = (chosen / counts[:, None] - inputs).astype(jnp.bfloat16)
        pieces.append(jnp.dot(differ, group_maps[group_idx], preferred_element_type=jnp.float32))
    pool_out = (jnp.concatenate(pieces, axis=1) * scales).astype(jnp.bfloat16)
    head_count = decay_rate.shape[0]
    head_dim = query_bf.shape[1] // head_count
    queries = rotate(query_bf.astype(jnp.float32).reshape(length, head_count, head_dim), positions)
    keys_in = rotate(
        key_bf.astype(jnp.float32).reshape(length, head_count, head_dim), positions
    ) * head_dim ** (-0.5)
    values_in = value_bf.astype(jnp.float32).reshape(length, head_count, head_dim)
    zeros_state = jnp.zeros((head_count, head_dim, head_dim), jnp.float32)
    local_output, local_state = block_retention(
        queries, keys_in, values_in, decay_rate, zeros_state
    )
    span_decay = jnp.exp(-decay_rate * length)
    whole_start = lax.all_gather(start_state, "sp", axis=2, tiled=True)[0]
    span_factor, carried_over = carried_in(
        (span_decay, local_state), "sp", combine_states, (jnp.ones_like(span_decay), zeros_state)
    )
    offset_float = (sp_index * length).astype(jnp.float32)
    carried_over = carried_over + jnp.exp(-decay_rate * offset_float)[:, None, None] * whole_start
    steps_in = jnp.arange(length, dtype=jnp.float32) + 1.0
    query_rows_scaled = queries * jnp.exp(-steps_in[:, None] * decay_rate[None, :])[:, :, None]
    retained_output = local_output + jnp.einsum(
        "lpi,pib->lpb", query_rows_scaled, carried_over, precision=highest_precision
    )
    retained_output = retained_output * lax.rsqrt(
        jnp.mean(retained_output * retained_output, axis=-1, keepdims=True) + eps
    )
    ret_out = retained_output.reshape(length, head_count * head_dim).astype(jnp.bfloat16)
    pool_cols, retention_cols = (
        lax.all_gather(pool_back, ("sp", "fs"), axis=1, tiled=True),
        lax.all_gather(retention_back, ("sp", "fs"), axis=1, tiled=True),
    )
    weight_local = jnp.concatenate([pool_cols, retention_cols], axis=0)
    joined = jnp.concatenate([pool_out, ret_out], axis=1)
    mixed = lax.psum_scatter(
        jnp.dot(joined, weight_local, preferred_element_type=jnp.float32).astype(jnp.bfloat16),
        "tp",
        scatter_dimension=0,
        tiled=True,
    )
    return mixed[None]


MESH = pl.DeviceIdType.MESH
LAG = 2
ORDER = (0, 3, 1, 2)


def where_am_i():
    sp, fs, tp = (lax.axis_index(name) for name in ("sp", "fs", "tp"))
    return sp, fs // 2, fs % 2, tp


def at(z, y, x, p):
    return (z, 2 * y + x, p)


def remote(src, dst, send, recv, target):
    return pltpu.make_async_remote_copy(
        src_ref=src, dst_ref=dst, send_sem=send, recv_sem=recv, device_id=target, device_id_type=MESH
    )


def piece(index, size):
    return pl.ds(pl.multiple_of(index * size, size), size)


def fused_kernel(
    tok, gain, wp, wq, wk, wv, state, pb, rb, pmap, pscale, rate, cos_t, sin_t,
    out,
    xt, xn, xg, wg, obuf, rbuf, backs, gv, st, stb, start, cosv, sinv, mapv, scv,
    krot, pool, mask, yb, yg, keep, give, take, done,
    l_sem, wl_sem, bl_sem, wy_send, wx_send, wf_send, w_recv,
    xz_send, xy_send, xp_send, x_recv,
    s_send, s_recv, b_send, b_recv, r_send, r_recv,
    h_send, c_send, y_recv, g_send, g_recv, o_send, o_recv,
):
    f32, bf = jnp.float32, jnp.bfloat16
    z, y, x, p = where_am_i()
    nz = 4
    half, width = xt.shape
    span = 2 * half
    feats = width // nz
    rows = wp.shape[0]
    group = wp.shape[1] // 2
    steps = 4 * nz
    mats = (wk, wq, wv, wp)
    fs = 2 * y + x
    me = at(z, y, x, p)
    partner = at(z, y, x, 1 - p)
    ypeer = at(z, 1 - y, x, p)
    xpeer = at(z, y, 1 - x, p)
    head = 2 * p + y

    barrier = pltpu.get_barrier_semaphore()
    others = [partner, xpeer]
    for dz in range(nz):
        for dy in range(2):
            if dz or dy:
                others.append(at((z + dz) % nz, (y + dy) % 2, x, p))
    for other in others:
        pl.semaphore_signal(barrier, inc=1, device_id=other, device_id_type=MESH)

    loads = [
        pltpu.make_async_copy(tok.at[piece(p, half)], xt, l_sem.at[0]),
        pltpu.make_async_copy(gain, gv, l_sem.at[1]),
        pltpu.make_async_copy(state, st, l_sem.at[2]),
        pltpu.make_async_copy(cos_t, cosv, l_sem.at[3]),
        pltpu.make_async_copy(sin_t, sinv, l_sem.at[4]),
        pltpu.make_async_copy(pmap.at[head], mapv, l_sem.at[5]),
        pltpu.make_async_copy(pscale.at[head], scv, l_sem.at[6]),
    ]
    for c in loads:
        c.start()
    own_w = []
    for m in range(4):
        c = pltpu.make_async_copy(mats[m].at[:, piece(y, group)], wg.at[m, piece(fs, rows)], wl_sem.at[m])
        c.start()
        own_w.append(c)
    loads[0].wait()
    loads[1].wait()

    block = 16
    for i in range(half // block):
        floats = xt[i * block : (i + 1) * block, :].astype(f32)
        xn[i * block : (i + 1) * block, :] = (
            floats * lax.rsqrt(jnp.mean(floats * floats, axis=-1, keepdims=True) + eps) * gv[...]
        ).astype(bf)

    def slot(ref, s, c, h):
        return ref.at[s, pl.ds(pl.multiple_of(c * span + h * half, half), half)]

    pl.semaphore_wait(barrier, len(others))

    sent = []

    def go(c):
        c.start()
        sent.append(c)

    def w_y(m):
        go(remote(mats[m].at[:, piece(1 - y, group)], wg.at[m, piece(fs, rows)], wy_send.at[m], w_recv.at[m, fs], ypeer))

    def w_x(m):
        go(remote(mats[m].at[:, piece(y, group)], wg.at[m, piece(fs, rows)], wx_send.at[m], w_recv.at[m, fs], xpeer))

    def w_wait(m, f):
        view = wg.at[m, piece(f, rows)]
        remote(view, view, wf_send.at[m], w_recv.at[m, f], partner).wait_recv()

    fy = 2 * (1 - y) + x

    def w_relay(m):
        w_wait(m, fy)
        view = wg.at[m, piece(fy, rows)]
        return remote(view, view, wf_send.at[m], w_recv.at[m, fy], xpeer)

    hi = z // 2
    zz = z * (1 - hi) + (3 - z) * hi
    near = [o * (1 - hi) + (3 - o) * hi for o in (1 - zz, 2, 3)]

    w_y(0)
    w_x(0)
    for i, c in enumerate(near):
        go(remote(xn.at[:, piece(c, feats)], slot(xg, y, z, p), xz_send.at[i], x_recv.at[y, z, p], at(c, y, x, p)))
    xg[y, pl.ds(pl.multiple_of(z * span + p * half, half), half), :] = xn[:, piece(z, feats)]

    def x_wait(s, c, h):
        view = slot(xg, s, c, h)
        remote(view, view, xp_send.at[0], x_recv.at[s, c, h], partner).wait_recv()

    def x_to_y(i, c):
        view = slot(xg, y, c, p)
        go(remote(view, view, xy_send.at[i], x_recv.at[y, c, p], ypeer))

    def x_to_partner(i, s, c):
        view = slot(xg, s, c, p)
        go(remote(view, view, xp_send.at[i], x_recv.at[s, c, p], partner))

    go(remote(xn.at[:, piece(z, feats)], slot(xg, y, z, p), xy_send.at[3], x_recv.at[y, z, p], ypeer))
    go(remote(xn.at[:, piece(z, feats)], slot(xg, y, z, p), xp_send.at[3], x_recv.at[y, z, p], partner))

    loads[2].wait()
    for j in range(2):
        stb[j] = st[j].astype(bf)
    toward = 3 * ((y + p) % 2)
    rs = st.shape[1]
    for j in range(2):
        same = (z == toward) & (y == j)
        dst = start.at[piece(z, rs)]

        @pl.when(same)
        def _():
            pltpu.make_async_copy(stb.at[j], dst, s_recv.at[z]).start()

        @pl.when(jnp.logical_not(same))
        def _():
            remote(stb.at[j], dst, s_send.at[j], s_recv.at[z], at(toward, j, x, p)).start()

    go(w_relay(0))
    w_x(1)
    x_wait(y, near[0], p)
    x_to_y(0, near[0])
    x_to_partner(0, y, near[0])
    w_y(1)
    x_wait(1 - y, z, p)
    x_to_partner(4 + 3, 1 - y, z)
    x_wait(y, near[1], p)
    x_to_y(1, near[1])
    x_to_partner(1, y, near[1])
    x_wait(1 - y, near[0], p)
    x_to_partner(4 + 0, 1 - y, near[0])
    go(w_relay(1))
    w_x(2)
    w_x(3)
    x_wait(y, near[2], p)
    x_to_y(2, near[2])
    x_to_partner(2, y, near[2])
    w_y(2)
    w_y(3)

    own_b = []
    for b, back in enumerate((pb, rb)):
        c = pltpu.make_async_copy(back, backs.at[b, :, piece(fs, rows)], bl_sem.at[b])
        c.start()
        own_b.append(c)
    for b, back in enumerate((pb, rb)):
        view = backs.at[b, :, piece(fs, rows)]
        first, second = ((xpeer, ypeer), (ypeer, xpeer))[b]
        go(remote(back, view, b_send.at[b, 0], b_recv.at[b, fs], first))
        go(remote(back, view, b_send.at[b, 1], b_recv.at[b, fs], second))
    fx = 2 * y + 1 - x
    fd = 2 * (1 - y) + 1 - x

    def b_wait(b, f):
        view = backs.at[b, :, piece(f, rows)]
        remote(view, view, b_send.at[b, 2], b_recv.at[b, f], partner).wait_recv()

    def b_relay(b):
        f, second = ((fx, ypeer), (fy, xpeer))[b]
        view = backs.at[b, :, piece(f, rows)]
        return remote(view, view, b_send.at[b, 2], b_recv.at[b, f], second)

    x_wait(1 - y, near[1], p)
    x_to_partner(4 + 1, 1 - y, near[1])
    x_wait(1 - y, near[2], p)
    x_to_partner(4 + 2, 1 - y, near[2])

    r = rate[y]
    row = lax.broadcasted_iota(jnp.int32, (span, span), 0)
    col = lax.broadcasted_iota(jnp.int32, (span, span), 1)
    gap = row - col
    for k in range(nz):
        dist = (gap + k * span).astype(f32)
        value = jnp.exp(-jnp.maximum(dist, 0.0) * r)
        mask[k] = jnp.where(dist >= 0.0, value, 0.0) if k == 0 else value
    loads[3].wait()
    loads[4].wait()
    loads[5].wait()
    loads[6].wait()

    for s in (y, 1 - y):
        for c in range(nz):
            x_wait(s, c, 1 - p)

    sems = (r_send, r_recv)

    def step(d, j):
        m, cc = j // nz, j % nz
        c = (nz - 1) - cc if d == 0 else cc
        s = p if d == 0 else 1 - p
        begins = (z == nz - 1) if d == 0 else (z == 0)
        ends = (z == 0) if d == 0 else (z == nz - 1)
        nxt = z - 1 if d == 0 else z + 1
        acc = jnp.dot(xg[s, piece(c, span), :], wg[m], preferred_element_type=f32)
        send, recv = r_send.at[d, j], r_recv.at[d, j]

        @pl.when(begins)
        def _():
            obuf[d, j] = acc.astype(bf)

        @pl.when(jnp.logical_not(begins))
        def _():
            remote(rbuf.at[d, j], rbuf.at[d, j], send, recv, partner).wait_recv()
            obuf[d, j] = (acc + rbuf[d, j].astype(f32)).astype(bf)

        @pl.when(jnp.logical_not(ends))
        def _():
            remote(obuf.at[d, j], rbuf.at[d, j], send, recv, at(nxt, y, x, p)).start()

    def body(k, carry):
        @pl.when(k == 2)
        def _():
            w_relay(2).start()

        @pl.when(k == 4)
        def _():
            w_relay(3).start()

        @pl.when(k == 8)
        def _():
            for b in range(2):
                b_wait(b, (fx, fy)[b])
                b_relay(b).start()

        lead = k - LAG * zz

        @pl.when((lead >= 0) & (lead < steps) & (lead % nz == 0))
        def _():
            m = lead // nz
            pltpu.make_async_copy(wp.at[:, piece(y, group)], wg.at[m, piece(fs, rows)], wl_sem.at[m]).wait()
            w_wait(m, fx)
            w_wait(m, fd)

        for d, j in ((0, k - LAG * (nz - 1 - z)), (1, k - LAG * z)):

            @pl.when((j >= 0) & (j < steps))
            def _():
                step(d, j)

        return carry

    lax.fori_loop(0, steps + LAG * (nz - 1), body, 0)

    owner = ((z == 0) & (y == p)) | ((z == nz - 1) & (y != p))
    is_end = (z == 0) | (z == nz - 1)
    flow = (y + p) % 2
    hop = z * (1 - flow) + (nz - 1 - z) * flow
    onward = at(z + 1 - 2 * flow, y, x, p)

    def chain(b, q, c):
        view = yg.at[b, q, c]
        return remote(view, view, c_send.at[b, q, c], y_recv.at[b, q, c], onward)

    @pl.when(is_end)
    def _():
        for k in range(nz):
            view = start.at[piece(k, rs)]
            remote(view, view, s_send.at[0], s_recv.at[k], partner).wait_recv()
        d = z // (nz - 1)
        small = group // 2

        def value_at(m, c):
            cc = (nz - 1 - c) * (1 - d) + c * d
            return obuf[d, m * nz + cc]

        pool[0:HALO, :] = jnp.zeros((HALO, group), bf)
        for c in range(nz):
            cosine, sine = cosv[c * span : (c + 1) * span, :], sinv[c * span : (c + 1) * span, :]
            k_c = value_at(0, c).astype(f32)
            a, b = k_c[:, :small], k_c[:, small:]
            scale = group ** (-0.5)
            krot[c * span : (c + 1) * span, :small] = ((a * cosine - b * sine) * scale).astype(bf)
            krot[c * span : (c + 1) * span, small:] = ((a * sine + b * cosine) * scale).astype(bf)
            pool[HALO + c * span : HALO + (c + 1) * span, :] = value_at(3, c)
        window = 2 * (1 + y) * (1 + 3 * p)
        brow = lax.broadcasted_iota(jnp.int32, (span, span + HALO), 0)
        bcol = lax.broadcasted_iota(jnp.int32, (span, span + HALO), 1)
        behind = brow + HALO - bcol
        band = jnp.where((behind >= 0) & (behind < window), 1.0, 0.0).astype(bf)
        place = lax.broadcasted_iota(jnp.int32, (span, 1), 0)
        for c in ORDER:
            cosine, sine = cosv[c * span : (c + 1) * span, :], sinv[c * span : (c + 1) * span, :]
            q_c = value_at(1, c).astype(f32)
            a, b = q_c[:, :small], q_c[:, small:]
            rq = jnp.concatenate([a * cosine - b * sine, a * sine + b * cosine], axis=-1)
            fade = jnp.exp(-((place + c * span).astype(f32) + 1.0) * r)
            acc = jnp.dot((rq * fade).astype(bf), start[...], preferred_element_type=f32)
            rq = rq.astype(bf)
            for e in range(c + 1):
                scores = lax.dot_general(
                    rq, krot[e * span : (e + 1) * span, :], (((1,), (1,)), ((), ())), preferred_element_type=f32
                )
                scores = (scores * mask[c - e]).astype(bf)
                acc += jnp.dot(scores, value_at(2, e), preferred_element_type=f32)
            ret = (acc * lax.rsqrt(jnp.mean(acc * acc, axis=-1, keepdims=True) + eps)).astype(bf)
            rows_c = pool[c * span : (c + 1) * span + HALO, :]
            trail = jnp.dot(band, rows_c, preferred_element_type=f32)
            counts = jnp.minimum(window, place + c * span + 1).astype(f32)
            differ = (trail / counts - value_at(3, c).astype(f32)).astype(bf)
            pooled = (jnp.dot(differ, mapv[...], preferred_element_type=f32) * scv[...]).astype(bf)

            @pl.when(owner)
            def _():
                yg[1, y, c] = ret
                yg[0, y, c] = pooled
                chain(1, y, c).start()
                chain(0, y, c).start()

            @pl.when(jnp.logical_not(owner))
            def _():
                yb[1, c] = ret
                yb[0, c] = pooled
                for b in (1, 0):
                    remote(yb.at[b, c], yg.at[b, y, c], h_send.at[b, c], y_recv.at[b, y, c], ypeer).start()

    for b in range(2):
        own_b[b].wait()
        b_wait(b, (fy, fx)[b])
        b_wait(b, fd)

    def arrive(b, q, c):
        view = yg.at[b, q, c]
        remote(view, view, c_send.at[b, q, c], y_recv.at[b, q, c], partner).wait_recv()

    def collect(c):
        for q in (y, 1 - y):
            for b in (1, 0):
                if q is y:

                    @pl.when(hop > 0)
                    def _():
                        arrive(b, q, c)

                        @pl.when(hop < nz - 1)
                        def _():
                            chain(b, q, c).start()
                else:
                    arrive(b, q, c)

                    @pl.when(hop < nz - 1)
                    def _():
                        chain(b, q, c).start()

    across = backs.shape[2]

    def multiply(c):
        acc = jnp.zeros((span, across), f32)
        for b in range(2):
            for q in range(2):
                acc += jnp.dot(
                    yg[b, q, c], backs[b, q * group : (q + 1) * group, :], preferred_element_type=f32
                )
        keep[c] = acc
        give[c] = keep[c, piece(1 - p, half), :].astype(bf)
        move = remote(give.at[c], take.at[c], g_send.at[c], g_recv.at[c], partner)
        move.start()
        return move

    def finish(c, move):
        move.wait()
        done[c] = (keep[c, piece(p, half), :] + take[c].astype(f32)).astype(bf)
        dst = out.at[:, piece(z, across)]

        @pl.when(z == c)
        def _():
            pltpu.make_async_copy(done.at[c], dst, o_recv.at[z]).start()

        @pl.when(z != c)
        def _():
            remote(done.at[c], dst, o_send.at[c], o_recv.at[z], at(c, y, x, p)).start()

    moves = []
    for i, c in enumerate(ORDER):
        collect(c)
        moves.append(multiply(c))
        if i:
            finish(ORDER[i - 1], moves[i - 1])
    finish(ORDER[-1], moves[-1])

    for k in range(nz):
        view = out.at[:, k * across : (k + 1) * across]
        remote(done.at[k], view, o_send.at[k], o_recv.at[k], partner).wait_recv()

        @pl.when(z != k)
        def _():
            remote(done.at[k], view, o_send.at[k], o_recv.at[k], partner).wait_send()

    @pl.when(hop < nz - 1)
    def _():
        for b in range(2):
            for q in range(2):
                for c in range(nz):
                    chain(b, q, c).wait_send()

    @pl.when(is_end & jnp.logical_not(owner))
    def _():
        for b in range(2):
            for c in range(nz):
                remote(yb.at[b, c], yb.at[b, c], h_send.at[b, c], y_recv.at[b, 0, c], partner).wait_send()

    for d in range(2):

        @pl.when((z > 0) if d == 0 else (z < nz - 1))
        def _():
            def drain(j, carry):
                remote(obuf.at[d, j], rbuf.at[d, j], r_send.at[d, j], r_recv.at[d, j], partner).wait_send()
                return carry

            lax.fori_loop(0, steps, drain, 0)

    for j in range(2):

        @pl.when(jnp.logical_not((z == toward) & (y == j)))
        def _():
            remote(stb.at[j], stb.at[j], s_send.at[j], s_recv.at[0], partner).wait_send()

    for m in (2, 3):
        view = wg.at[m, piece(fy, rows)]
        remote(view, view, wf_send.at[m], w_recv.at[m, fy], partner).wait_send()
    for b in range(2):
        b_relay(b).wait_send()
    for c in sent:
        c.wait_send()


def rotary_tables(length, half_dim):
    inv_freq = np.float32(1.0) / np.power(
        np.float32(rope_base), np.linspace(0.0, 1.0, half_dim, dtype=np.float32)
    )
    angles = np.arange(length, dtype=np.float32)[:, None] * inv_freq[None, :].astype(np.float32)
    return np.cos(angles).astype(np.float32), np.sin(angles).astype(np.float32)


def paired(
    tokens, norm_gain, pool_proj, query_proj, key_proj, value_proj, pool_map, pool_scale,
    decay_rate, start_state, pool_back, retention_back,
):
    bf, f32 = jnp.bfloat16, jnp.float32
    nsp = lax.axis_size("sp")
    tok = tokens[0]
    span, width = tok.shape
    rows, two = pool_proj.shape
    group = two // 2
    length = nsp * span
    half = span // 2
    rs = start_state.shape[2]
    steps = 4 * nsp
    across = 4 * pool_back.shape[1]
    vm, hbm = pl.BlockSpec(memory_space=pltpu.VMEM), pl.BlockSpec(memory_space=pl.ANY)
    dma = pltpu.SemaphoreType.DMA
    cosine, sine = rotary_tables(length, group // 2)
    return pl.pallas_call(
        fused_kernel,
        out_shape=jax.ShapeDtypeStruct((half, width), bf),
        in_specs=[hbm] * 11 + [pl.BlockSpec(memory_space=pltpu.SMEM)] + [hbm] * 2,
        out_specs=vm,
        scratch_shapes=[
            pltpu.VMEM((half, width), bf),
            pltpu.VMEM((half, width), bf),
            pltpu.VMEM((2, length, width // nsp), bf),
            pltpu.VMEM((4, 4 * rows, group), bf),
            pltpu.VMEM((2, steps, span, group), bf),
            pltpu.VMEM((2, steps, span, group), bf),
            pltpu.VMEM((2, pool_back.shape[0], across), bf),
            pltpu.VMEM((1, width), f32),
            pltpu.VMEM((2, rs, group), f32),
            pltpu.VMEM((2, rs, group), bf),
            pltpu.VMEM((nsp * rs, group), bf),
            pltpu.VMEM((length, group // 2), f32),
            pltpu.VMEM((length, group // 2), f32),
            pltpu.VMEM((group, group), bf),
            pltpu.VMEM((1, group), f32),
            pltpu.VMEM((length, group), bf),
            pltpu.VMEM((HALO + length, group), bf),
            pltpu.VMEM((nsp, span, span), f32),
            pltpu.VMEM((2, nsp, span, group), bf),
            pltpu.VMEM((2, 2, nsp, span, group), bf),
            pltpu.VMEM((nsp, span, across), f32),
            pltpu.VMEM((nsp, half, across), bf),
            pltpu.VMEM((nsp, half, across), bf),
            pltpu.VMEM((nsp, half, across), bf),
            dma((7,)), dma((4,)), dma((2,)), dma((4,)), dma((4,)), dma((4,)), dma((4, 4)),
            dma((3,)), dma((4,)), dma((8,)), dma((2, nsp, 2)),
            dma((2,)), dma((nsp,)), dma((2, 3)), dma((2, 4)), dma((2, steps)), dma((2, steps)),
            dma((2, nsp)), dma((2, 2, nsp)), dma((2, 2, nsp)), dma((nsp,)), dma((nsp,)), dma((nsp,)), dma((nsp,)),
        ],
        compiler_params=pltpu.CompilerParams(collective_id=0, has_side_effects=True, vmem_limit_bytes=60 * 2**20),
        name="fused",
    )(
        tok, norm_gain[None, :], pool_proj, query_proj, key_proj, value_proj,
        start_state[0], pool_back, retention_back, pool_map,
        pool_scale.reshape(pool_map.shape[0], 1, group), decay_rate, jnp.asarray(cosine), jnp.asarray(sine),
    )[None]


def solution(mesh):
    sizes = mesh.shape
    small = sizes["sp"] == 4 and sizes["fs"] == 4 and sizes["tp"] == 2
    placed = (
        P("fs", "sp", None),
        P(),
        P(("sp", "fs"), "tp"),
        P(("sp", "fs"), "tp"),
        P(("sp", "fs"), "tp"),
        P(("sp", "fs"), "tp"),
        P(),
        P(),
        P("tp"),
        P("fs", "tp", "sp", None),
        P("tp", ("sp", "fs")),
        P("tp", ("sp", "fs")),
    )
    return jax.shard_map(
        paired if small else on_device,
        mesh=mesh,
        in_specs=placed,
        out_specs=P("fs", ("sp", "tp"), None),
        check_vma=False,
    )
```

time: 146 us -> 119 us (0.82)
  the two profiles are of different devices: /device:TPU:29 before, /device:TPU:23 now
where the time goes in v1:
time: 119 us
  Pallas kernels  117 us (98%)
  local copies, waits for them, and re-layouts  1.87 us (2%)
    pallas_call x1, Pallas kernels, paired(): pl.pallas_call(fused_kernel, out_shape=jax.ShapeDtypeStruct((half, width)...  117 us

profile of v1, /device:TPU:23, one launch (start us, length us, event | category | flops | bytes accessed | tf_op | source)
XLA Modules:
  0.0 119.3 jit_solution(12324372248268088437)
XLA Ops:
  0.0 117.4 %fused.1 = bf16[64,4096]{1,0:T(8,128)(2,1)} custom-call(bf16[128,4096]{1,0:T(8,128)(2,1)} %bitcast.6, f32[1,4096]{1,0:T(1,128)} %bitcast.8, bf16[256,512]{1,0:T(8,128)(2,1)} %wp.1, bf16[256,512]{1,0:T(8,128)(2,1)} %wq.1, bf16[256,512]{1,0:T(8,128)(2,1)} %wk.1, bf16[256,512]{1,0:T(8,128)(2,1)} %wv.1, f32[2,64,256]{2,1,0:T(8,128)} %bitcast.7, ...), custom_call_target="tpu_custom_call" | custom-call | tf_op jit(solution)/shard_map/fused/pallas_call | solution.py:718
  117.4 1.9 %copy.16 = bf16[1,64,4096]{2,1,0:T(8,128)(2,1)} copy(bf16[1,64,4096]{2,1,0:T(8,128)(2,1)} %bitcast.5) | data formatting | bytes 1048576

commit v2 on v1

--- a/solution.py
+++ b/solution.py
@@ -227,7 +227,11 @@
 
 
 MESH = pl.DeviceIdType.MESH
-LAG = 2
+LAG_E = 2
+LAG_L = 3
+LATE = 4
+LATE_MATS = (0, 1, 0, 1, 2, 2, 0, 1, 2, 3, 3, 3, 0, 1, 2, 3)
+LATE_CHUNKS = (0, 0, 1, 1, 0, 1, 2, 2, 2, 0, 1, 2, 3, 3, 3, 3)
 ORDER = (0, 3, 1, 2)
 
 
@@ -326,8 +330,11 @@
     def w_y(m):
         go(remote(mats[m].at[:, piece(1 - y, group)], wg.at[m, piece(fs, rows)], wy_send.at[m], w_recv.at[m, fs], ypeer))
 
+    def w_copy_x(m):
+        return remote(mats[m].at[:, piece(y, group)], wg.at[m, piece(fs, rows)], wx_send.at[m], w_recv.at[m, fs], xpeer)
+
     def w_x(m):
-        go(remote(mats[m].at[:, piece(y, group)], wg.at[m, piece(fs, rows)], wx_send.at[m], w_recv.at[m, fs], xpeer))
+        go(w_copy_x(m))
 
     def w_wait(m, f):
         view = wg.at[m, piece(f, rows)]
@@ -343,6 +350,11 @@
     hi = z // 2
     zz = z * (1 - hi) + (3 - z) * hi
     near = [o * (1 - hi) + (3 - o) * hi for o in (1 - zz, 2, 3)]
+    flow = (y + p) % 2
+    hop_e = (nz - 1 - z) * (1 - flow) + z * flow
+    hop_l = nz - 1 - hop_e
+    toward_e = at(z - 1 + 2 * flow, y, x, p)
+    toward_l = at(z + 1 - 2 * flow, y, x, p)
 
     w_y(0)
     w_x(0)
@@ -360,10 +372,13 @@
 
     def x_to_partner(i, s, c):
         view = slot(xg, s, c, p)
-        go(remote(view, view, xp_send.at[i], x_recv.at[s, c, p], partner))
-
+        return remote(view, view, xp_send.at[i], x_recv.at[s, c, p], partner)
+
+    w_y(1)
+    w_x(1)
+    go(remote(xn.at[:, piece(z, feats)], slot(xg, y, z, p), xp_send.at[3], x_recv.at[y, z, p], partner))
     go(remote(xn.at[:, piece(z, feats)], slot(xg, y, z, p), xy_send.at[3], x_recv.at[y, z, p], ypeer))
-    go(remote(xn.at[:, piece(z, feats)], slot(xg, y, z, p), xp_send.at[3], x_recv.at[y, z, p], partner))
+    w_y(2)
 
     loads[2].wait()
     for j in range(2):
@@ -382,55 +397,6 @@
         def _():
             remote(stb.at[j], dst, s_send.at[j], s_recv.at[z], at(toward, j, x, p)).start()
 
-    go(w_relay(0))
-    w_x(1)
-    x_wait(y, near[0], p)
-    x_to_y(0, near[0])
-    x_to_partner(0, y, near[0])
-    w_y(1)
-    x_wait(1 - y, z, p)
-    x_to_partner(4 + 3, 1 - y, z)
-    x_wait(y, near[1], p)
-    x_to_y(1, near[1])
-    x_to_partner(1, y, near[1])
-    x_wait(1 - y, near[0], p)
-    x_to_partner(4 + 0, 1 - y, near[0])
-    go(w_relay(1))
-    w_x(2)
-    w_x(3)
-    x_wait(y, near[2], p)
-    x_to_y(2, near[2])
-    x_to_partner(2, y, near[2])
-    w_y(2)
-    w_y(3)
-
-    own_b = []
-    for b, back in enumerate((pb, rb)):
-        c = pltpu.make_async_copy(back, backs.at[b, :, piece(fs, rows)], bl_sem.at[b])
-        c.start()
-        own_b.append(c)
-    for b, back in enumerate((pb, rb)):
-        view = backs.at[b, :, piece(fs, rows)]
-        first, second = ((xpeer, ypeer), (ypeer, xpeer))[b]
-        go(remote(back, view, b_send.at[b, 0], b_recv.at[b, fs], first))
-        go(remote(back, view, b_send.at[b, 1], b_recv.at[b, fs], second))
-    fx = 2 * y + 1 - x
-    fd = 2 * (1 - y) + 1 - x
-
-    def b_wait(b, f):
-        view = backs.at[b, :, piece(f, rows)]
-        remote(view, view, b_send.at[b, 2], b_recv.at[b, f], partner).wait_recv()
-
-    def b_relay(b):
-        f, second = ((fx, ypeer), (fy, xpeer))[b]
-        view = backs.at[b, :, piece(f, rows)]
-        return remote(view, view, b_send.at[b, 2], b_recv.at[b, f], second)
-
-    x_wait(1 - y, near[1], p)
-    x_to_partner(4 + 1, 1 - y, near[1])
-    x_wait(1 - y, near[2], p)
-    x_to_partner(4 + 2, 1 - y, near[2])
-
     r = rate[y]
     row = lax.broadcasted_iota(jnp.int32, (span, span), 0)
     col = lax.broadcasted_iota(jnp.int32, (span, span), 1)
@@ -439,79 +405,146 @@
         dist = (gap + k * span).astype(f32)
         value = jnp.exp(-jnp.maximum(dist, 0.0) * r)
         mask[k] = jnp.where(dist >= 0.0, value, 0.0) if k == 0 else value
-    loads[3].wait()
-    loads[4].wait()
-    loads[5].wait()
-    loads[6].wait()
-
-    for s in (y, 1 - y):
-        for c in range(nz):
+    for c in loads[3:]:
+        c.wait()
+
+    x_wait(y, near[0], p)
+    x_to_y(0, near[0])
+    go(x_to_partner(0, y, near[0]))
+    go(w_relay(0))
+    w_y(3)
+    go(w_relay(1))
+    w_x(2)
+    x_wait(y, near[1], p)
+    x_to_y(1, near[1])
+    go(x_to_partner(1, y, near[1]))
+    x_wait(1 - y, z, p)
+    go(x_to_partner(4 + 3, 1 - y, z))
+
+    own_b = []
+    for b, back in enumerate((pb, rb)):
+        c = pltpu.make_async_copy(back, backs.at[b, :, piece(fs, rows)], bl_sem.at[b])
+        c.start()
+        own_b.append(c)
+    fx = 2 * y + 1 - x
+    fd = 2 * (1 - y) + 1 - x
+
+    def b_own(b, i):
+        back = (pb, rb)[b]
+        target = ((xpeer, ypeer), (ypeer, xpeer))[b][i]
+        return remote(back, backs.at[b, :, piece(fs, rows)], b_send.at[b, i], b_recv.at[b, fs], target)
+
+    def b_wait(b, f):
+        view = backs.at[b, :, piece(f, rows)]
+        remote(view, view, b_send.at[b, 2], b_recv.at[b, f], partner).wait_recv()
+
+    def b_relay(b):
+        f, second = ((fx, ypeer), (fy, xpeer))[b]
+        view = backs.at[b, :, piece(f, rows)]
+        return remote(view, view, b_send.at[b, 2], b_recv.at[b, f], second)
+
+    def listed(table, j):
+        word = sum(v << (2 * i) for i, v in enumerate(table))
+        word = word - 2**32 if word >= 2**31 else word
+        return lax.shift_right_logical(jnp.int32(word), 2 * j) & 3
+
+    def step(e, m, i):
+        d = flow if e == 0 else 1 - flow
+        hop = hop_e if e == 0 else hop_l
+        s = y if e == 0 else 1 - y
+        c = (nz - 1 - i) * (1 - d) + i * d
+        at_slot = m * nz + c
+
+        @pl.when(m == 0)
+        def _():
             x_wait(s, c, 1 - p)
 
-    sems = (r_send, r_recv)
-
-    def step(d, j):
-        m, cc = j // nz, j % nz
-        c = (nz - 1) - cc if d == 0 else cc
-        s = p if d == 0 else 1 - p
-        begins = (z == nz - 1) if d == 0 else (z == 0)
-        ends = (z == 0) if d == 0 else (z == nz - 1)
-        nxt = z - 1 if d == 0 else z + 1
         acc = jnp.dot(xg[s, piece(c, span), :], wg[m], preferred_element_type=f32)
-        send, recv = r_send.at[d, j], r_recv.at[d, j]
-
-        @pl.when(begins)
-        def _():
-            obuf[d, j] = acc.astype(bf)
-
-        @pl.when(jnp.logical_not(begins))
-        def _():
-            remote(rbuf.at[d, j], rbuf.at[d, j], send, recv, partner).wait_recv()
-            obuf[d, j] = (acc + rbuf[d, j].astype(f32)).astype(bf)
-
-        @pl.when(jnp.logical_not(ends))
-        def _():
-            remote(obuf.at[d, j], rbuf.at[d, j], send, recv, at(nxt, y, x, p)).start()
+        send, recv = r_send.at[e, at_slot], r_recv.at[e, at_slot]
+
+        @pl.when(hop == 0)
+        def _():
+            obuf[e, at_slot] = acc.astype(bf)
+
+        @pl.when(hop > 0)
+        def _():
+            remote(rbuf.at[e, at_slot], rbuf.at[e, at_slot], send, recv, partner).wait_recv()
+            obuf[e, at_slot] = (acc + rbuf[e, at_slot].astype(f32)).astype(bf)
+
+        @pl.when(hop < nz - 1)
+        def _():
+            remote(
+                obuf.at[e, at_slot], rbuf.at[e, at_slot], send, recv, toward_e if e == 0 else toward_l
+            ).start()
+
+    def w_ready(m):
+        own_w[m].wait()
+        w_wait(m, fx)
+        w_wait(m, fd)
+
+    def event(k, when, act):
+        @pl.when(k == when)
+        def _():
+            act()
+
+    def a3():
+        x_wait(y, near[2], p)
+        view = slot(xg, y, near[2], p)
+        remote(view, view, xy_send.at[2], x_recv.at[y, near[2], p], ypeer).start()
+        x_to_partner(2, y, near[2]).start()
+
+    def b_next(i):
+        x_wait(1 - y, near[i], p)
+        x_to_partner(4 + i, 1 - y, near[i]).start()
+
+    def relay2():
+        w_relay(2).start()
+        w_copy_x(3).start()
+
+    def back_own():
+        for i in range(2):
+            for b in range(2):
+                b_own(b, i).start()
+
+    def back_relay():
+        for b in range(2):
+            b_wait(b, (fx, fy)[b])
+            b_relay(b).start()
 
     def body(k, carry):
-        @pl.when(k == 2)
-        def _():
-            w_relay(2).start()
-
-        @pl.when(k == 4)
-        def _():
-            w_relay(3).start()
-
-        @pl.when(k == 8)
-        def _():
-            for b in range(2):
-                b_wait(b, (fx, fy)[b])
-                b_relay(b).start()
-
-        lead = k - LAG * zz
-
-        @pl.when((lead >= 0) & (lead < steps) & (lead % nz == 0))
-        def _():
-            m = lead // nz
-            pltpu.make_async_copy(wp.at[:, piece(y, group)], wg.at[m, piece(fs, rows)], wl_sem.at[m]).wait()
-            w_wait(m, fx)
-            w_wait(m, fd)
-
-        for d, j in ((0, k - LAG * (nz - 1 - z)), (1, k - LAG * z)):
-
-            @pl.when((j >= 0) & (j < steps))
-            def _():
-                step(d, j)
+        event(k, 0, lambda: w_ready(0))
+        event(k, 2, a3)
+        event(k, 4, lambda: w_ready(1))
+        event(k, 4, relay2)
+        event(k, 5, lambda: b_next(0))
+        event(k, 7, lambda: w_relay(3).start())
+        event(k, 8, lambda: w_ready(2))
+        event(k, 9, lambda: b_next(1))
+        event(k, 10, lambda: b_next(2))
+        event(k, 10, back_own)
+        event(k, 12, lambda: w_ready(3))
+        event(k, 18, back_relay)
+
+        je = k - LAG_E * hop_e
+
+        @pl.when((je >= 0) & (je < steps))
+        def _():
+            step(0, je // nz, je % nz)
+
+        jl = k - LAG_L * hop_l - LATE
+
+        @pl.when((jl >= 0) & (jl < steps))
+        def _():
+            step(1, listed(LATE_MATS, jl), listed(LATE_CHUNKS, jl))
 
         return carry
 
-    lax.fori_loop(0, steps + LAG * (nz - 1), body, 0)
-
-    owner = ((z == 0) & (y == p)) | ((z == nz - 1) & (y != p))
+    lax.fori_loop(0, steps + LATE + LAG_L * (nz - 1), body, 0)
+
+    owner = hop_e == nz - 1
     is_end = (z == 0) | (z == nz - 1)
-    flow = (y + p) % 2
-    hop = z * (1 - flow) + (nz - 1 - z) * flow
-    onward = at(z + 1 - 2 * flow, y, x, p)
+    hop = hop_l
+    onward = toward_l
 
     def chain(b, q, c):
         view = yg.at[b, q, c]
@@ -522,12 +555,11 @@
         for k in range(nz):
             view = start.at[piece(k, rs)]
             remote(view, view, s_send.at[0], s_recv.at[k], partner).wait_recv()
-        d = z // (nz - 1)
+        e = hop_l // (nz - 1)
         small = group // 2
 
         def value_at(m, c):
-            cc = (nz - 1 - c) * (1 - d) + c * d
-            return obuf[d, m * nz + cc]
+            return obuf[e, m * nz + c]
 
         pool[0:HALO, :] = jnp.zeros((HALO, group), bf)
         for c in range(nz):
@@ -552,12 +584,12 @@
             fade = jnp.exp(-((place + c * span).astype(f32) + 1.0) * r)
             acc = jnp.dot((rq * fade).astype(bf), start[...], preferred_element_type=f32)
             rq = rq.astype(bf)
-            for e in range(c + 1):
+            for g in range(c + 1):
                 scores = lax.dot_general(
-                    rq, krot[e * span : (e + 1) * span, :], (((1,), (1,)), ((), ())), preferred_element_type=f32
+                    rq, krot[g * span : (g + 1) * span, :], (((1,), (1,)), ((), ())), preferred_element_type=f32
                 )
-                scores = (scores * mask[c - e]).astype(bf)
-                acc += jnp.dot(scores, value_at(2, e), preferred_element_type=f32)
+                scores = (scores * mask[c - g]).astype(bf)
+                acc += jnp.dot(scores, value_at(2, g), preferred_element_type=f32)
             ret = (acc * lax.rsqrt(jnp.mean(acc * acc, axis=-1, keepdims=True) + eps)).astype(bf)
             rows_c = pool[c * span : (c + 1) * span + HALO, :]
             trail = jnp.dot(band, rows_c, preferred_element_type=f32)
@@ -588,42 +620,37 @@
         view = yg.at[b, q, c]
         remote(view, view, c_send.at[b, q, c], y_recv.at[b, q, c], partner).wait_recv()
 
-    def collect(c):
-        for q in (y, 1 - y):
-            for b in (1, 0):
-                if q is y:
-
-                    @pl.when(hop > 0)
-                    def _():
-                        arrive(b, q, c)
-
-                        @pl.when(hop < nz - 1)
-                        def _():
-                            chain(b, q, c).start()
-                else:
-                    arrive(b, q, c)
-
-                    @pl.when(hop < nz - 1)
-                    def _():
-                        chain(b, q, c).start()
+    def pass_on(b, q, c):
+        arrive(b, q, c)
+
+        @pl.when(hop < nz - 1)
+        def _():
+            chain(b, q, c).start()
 
     across = backs.shape[2]
 
-    def multiply(c):
+    def product(q, c):
         acc = jnp.zeros((span, across), f32)
         for b in range(2):
-            for q in range(2):
-                acc += jnp.dot(
-                    yg[b, q, c], backs[b, q * group : (q + 1) * group, :], preferred_element_type=f32
-                )
-        keep[c] = acc
+            acc += jnp.dot(yg[b, q, c], backs[b, piece(q, group), :], preferred_element_type=f32)
+        return acc
+
+    def early(c):
+        @pl.when(hop > 0)
+        def _():
+            for b in (1, 0):
+                pass_on(b, y, c)
+
+    def give_copy(c):
+        return remote(give.at[c], take.at[c], g_send.at[c], g_recv.at[c], partner)
+
+    def multiply(c):
+        keep[c] = keep[c] + product(1 - y, c)
         give[c] = keep[c, piece(1 - p, half), :].astype(bf)
-        move = remote(give.at[c], take.at[c], g_send.at[c], g_recv.at[c], partner)
-        move.start()
-        return move
-
-    def finish(c, move):
-        move.wait()
+        give_copy(c).start()
+
+    def finish(c):
+        give_copy(c).wait_recv()
         done[c] = (keep[c, piece(p, half), :] + take[c].astype(f32)).astype(bf)
         dst = out.at[:, piece(z, across)]
 
@@ -635,13 +662,36 @@
         def _():
             remote(done.at[c], dst, o_send.at[c], o_recv.at[z], at(c, y, x, p)).start()
 
-    moves = []
+    for c in ORDER:
+        early(c)
+        keep[c] = product(y, c)
     for i, c in enumerate(ORDER):
-        collect(c)
-        moves.append(multiply(c))
-        if i:
-            finish(ORDER[i - 1], moves[i - 1])
-    finish(ORDER[-1], moves[-1])
+        for b in (1, 0):
+            pass_on(b, 1 - y, c)
+        multiply(c)
+
+        for late in range(3):
+            then = i - late
+            if late == 0 and then >= 0:
+
+                @pl.when(hop >= 2)
+                def _():
+                    finish(ORDER[then])
+            if late == 2 and then >= 0:
+
+                @pl.when(hop == 1)
+                def _():
+                    finish(ORDER[then])
+
+    @pl.when(hop == 1)
+    def _():
+        for c in ORDER[2:]:
+            finish(c)
+
+    @pl.when(hop == 0)
+    def _():
+        for c in ORDER:
+            finish(c)
 
     for k in range(nz):
         view = out.at[:, k * across : (k + 1) * across]
@@ -664,12 +714,12 @@
             for c in range(nz):
                 remote(yb.at[b, c], yb.at[b, c], h_send.at[b, c], y_recv.at[b, 0, c], partner).wait_send()
 
-    for d in range(2):
-
-        @pl.when((z > 0) if d == 0 else (z < nz - 1))
+    for e in range(2):
+
+        @pl.when((hop_e if e == 0 else hop_l) < nz - 1)
         def _():
             def drain(j, carry):
-                remote(obuf.at[d, j], rbuf.at[d, j], r_send.at[d, j], r_recv.at[d, j], partner).wait_send()
+                remote(obuf.at[e, j], rbuf.at[e, j], r_send.at[e, j], r_recv.at[e, j], partner).wait_send()
                 return carry
 
             lax.fori_loop(0, steps, drain, 0)
@@ -680,11 +730,21 @@
         def _():
             remote(stb.at[j], stb.at[j], s_send.at[j], s_recv.at[0], partner).wait_send()
 
+    for c in range(nz):
+        give_copy(c).wait_send()
     for m in (2, 3):
         view = wg.at[m, piece(fy, rows)]
         remote(view, view, wf_send.at[m], w_recv.at[m, fy], partner).wait_send()
     for b in range(2):
+        for i in range(2):
+            b_own(b, i).wait_send()
         b_relay(b).wait_send()
+    w_copy_x(3).wait_send()
+    for i in (2, 4, 5, 6):
+        view = slot(xg, y, z, p)
+        remote(view, view, xp_send.at[i], x_recv.at[y, z, p], partner).wait_send()
+    view = slot(xg, y, z, p)
+    remote(view, view, xy_send.at[2], x_recv.at[y, z, p], partner).wait_send()
     for c in sent:
         c.wait_send()
 

time: 119 us -> 96.2 us (0.81)
  the two profiles are of different devices: /device:TPU:23 before, /device:TPU:21 now
where the time goes in v2:
time: 96.2 us; the launch traced here: 96 us
  Pallas kernels  94.2 us (98%)
  local copies, waits for them, and re-layouts  1.87 us (2%)
    pallas_call x1, Pallas kernels, paired(): pl.pallas_call(fused_kernel, out_shape=jax.ShapeDtypeStruct((half, width)...  94.2 us

profile of v2, /device:TPU:21, one launch (start us, length us, event | category | flops | bytes accessed | tf_op | source)
XLA Modules:
  0.0 96.0 jit_solution(6840190758204761388)
XLA Ops:
  0.0 94.2 %fused.1 = bf16[64,4096]{1,0:T(8,128)(2,1)} custom-call(bf16[128,4096]{1,0:T(8,128)(2,1)} %bitcast.6, f32[1,4096]{1,0:T(1,128)} %bitcast.8, bf16[256,512]{1,0:T(8,128)(2,1)} %wp.1, bf16[256,512]{1,0:T(8,128)(2,1)} %wq.1, bf16[256,512]{1,0:T(8,128)(2,1)} %wk.1, bf16[256,512]{1,0:T(8,128)(2,1)} %wv.1, f32[2,64,256]{2,1,0:T(8,128)} %bitcast.7, ...), custom_call_target="tpu_custom_call" | custom-call | tf_op jit(solution)/shard_map/fused/pallas_call | solution.py:778
  94.2 1.9 %copy.16 = bf16[1,64,4096]{2,1,0:T(8,128)(2,1)} copy(bf16[1,64,4096]{2,1,0:T(8,128)(2,1)} %bitcast.5) | data formatting | bytes 1048576

commit v3 on v2

--- a/solution.py
+++ b/solution.py
@@ -227,12 +227,26 @@
 
 
 MESH = pl.DeviceIdType.MESH
-LAG_E = 2
-LAG_L = 3
-LATE = 4
-LATE_MATS = (0, 1, 0, 1, 2, 2, 0, 1, 2, 3, 3, 3, 0, 1, 2, 3)
-LATE_CHUNKS = (0, 0, 1, 1, 0, 1, 2, 2, 2, 0, 1, 2, 3, 3, 3, 3)
 ORDER = (0, 3, 1, 2)
+STEPS = (
+    (0, 0, 0, 10.0), (0, 0, 1, 10.7), (0, 1, 0, 14.0), (0, 1, 1, 14.7), (0, 0, 2, 15.4), (0, 1, 2, 16.1), (0, 0, 3, 16.8), (0, 1, 3, 17.5),
+    (1, 0, 1, 18.2), (1, 1, 1, 18.9), (0, 2, 0, 20.3), (0, 2, 1, 21.0), (0, 2, 2, 21.7), (0, 2, 3, 22.4),
+    (1, 2, 1, 23.1), (1, 0, 0, 23.8), (1, 1, 0, 24.5), (1, 2, 0, 25.2),
+    (0, 3, 0, 25.9), (0, 3, 1, 26.6), (0, 3, 2, 27.3), (0, 3, 3, 28.0),
+    (1, 0, 2, 28.7), (1, 1, 2, 29.4), (1, 2, 2, 30.1), (1, 0, 3, 30.8), (1, 1, 3, 31.5), (1, 2, 3, 32.2),
+    (1, 3, 0, 32.9), (1, 3, 1, 33.6), (1, 3, 2, 34.3), (1, 3, 3, 35.0),
+)
+HOP = 2.7
+NEAR = ((1, 2, 3), (0, 2, 3), (3, 1, 0), (2, 1, 0))
+
+
+def places(when, needs):
+    result = []
+    for hop in range(4):
+        due = [n for n, step in enumerate(STEPS) if step[3] + HOP * hop >= when] + [len(STEPS)]
+        used = [n for n, step in enumerate(STEPS) if needs(hop, *step[:3])] + [len(STEPS)]
+        result.append(min(due[0], used[0]))
+    return tuple(result)
 
 
 def where_am_i():
@@ -350,11 +364,10 @@
     hi = z // 2
     zz = z * (1 - hi) + (3 - z) * hi
     near = [o * (1 - hi) + (3 - o) * hi for o in (1 - zz, 2, 3)]
-    flow = (y + p) % 2
-    hop_e = (nz - 1 - z) * (1 - flow) + z * flow
-    hop_l = nz - 1 - hop_e
-    toward_e = at(z - 1 + 2 * flow, y, x, p)
-    toward_l = at(z + 1 - 2 * flow, y, x, p)
+    hop = (nz - 1 - z) * (1 - p) + z * p
+    toward = at(z - 1 + 2 * p, y, x, p)
+    onward = at(z + 1 - 2 * p, y, x, p)
+    goal = (nz - 1) * p
 
     w_y(0)
     w_x(0)
@@ -383,19 +396,18 @@
     loads[2].wait()
     for j in range(2):
         stb[j] = st[j].astype(bf)
-    toward = 3 * ((y + p) % 2)
     rs = st.shape[1]
     for j in range(2):
-        same = (z == toward) & (y == j)
-        dst = start.at[piece(z, rs)]
+        same = (z == goal) & (y == j)
+        dst = start.at[y, piece(z, rs)]
 
         @pl.when(same)
         def _():
-            pltpu.make_async_copy(stb.at[j], dst, s_recv.at[z]).start()
+            pltpu.make_async_copy(stb.at[j], dst, s_recv.at[y, z]).start()
 
         @pl.when(jnp.logical_not(same))
         def _():
-            remote(stb.at[j], dst, s_send.at[j], s_recv.at[z], at(toward, j, x, p)).start()
+            remote(stb.at[j], dst, s_send.at[j], s_recv.at[y, z], at(goal, j, x, p)).start()
 
     r = rate[y]
     row = lax.broadcasted_iota(jnp.int32, (span, span), 0)
@@ -415,12 +427,6 @@
     w_y(3)
     go(w_relay(1))
     w_x(2)
-    x_wait(y, near[1], p)
-    x_to_y(1, near[1])
-    go(x_to_partner(1, y, near[1]))
-    x_wait(1 - y, z, p)
-    go(x_to_partner(4 + 3, 1 - y, z))
-
     own_b = []
     for b, back in enumerate((pb, rb)):
         c = pltpu.make_async_copy(back, backs.at[b, :, piece(fs, rows)], bl_sem.at[b])
@@ -443,16 +449,23 @@
         view = backs.at[b, :, piece(f, rows)]
         return remote(view, view, b_send.at[b, 2], b_recv.at[b, f], second)
 
-    def listed(table, j):
-        word = sum(v << (2 * i) for i, v in enumerate(table))
-        word = word - 2**32 if word >= 2**31 else word
-        return lax.shift_right_logical(jnp.int32(word), 2 * j) & 3
-
-    def step(e, m, i):
-        d = flow if e == 0 else 1 - flow
-        hop = hop_e if e == 0 else hop_l
-        s = y if e == 0 else 1 - y
-        c = (nz - 1 - i) * (1 - d) + i * d
+    def by_place(values):
+        result = values[3]
+        for h in (2, 1, 0):
+            result = jnp.where(hop == h, values[h], result)
+        return result
+
+    def listed(table, n):
+        words = []
+        for part in (table[:16], table[16:]):
+            word = sum(v << (2 * i) for i, v in enumerate(part))
+            words.append(np.int32(word - 2**32 if word >= 2**31 else word))
+        return lax.shift_right_logical(jnp.where(n < 16, words[0], words[1]), 2 * (n % 16)) & 3
+
+    def step(n):
+        e, m, i = (listed([entry[k] for entry in STEPS], n) for k in range(3))
+        s = y + e * (1 - 2 * y)
+        c = (nz - 1 - i) * (1 - p) + i * p
         at_slot = m * nz + c
 
         @pl.when(m == 0)
@@ -473,29 +486,27 @@
 
         @pl.when(hop < nz - 1)
         def _():
-            remote(
-                obuf.at[e, at_slot], rbuf.at[e, at_slot], send, recv, toward_e if e == 0 else toward_l
-            ).start()
+            remote(obuf.at[e, at_slot], rbuf.at[e, at_slot], send, recv, toward).start()
 
     def w_ready(m):
         own_w[m].wait()
         w_wait(m, fx)
         w_wait(m, fd)
 
-    def event(k, when, act):
-        @pl.when(k == when)
+    def event(n, when, act):
+        @pl.when(n == by_place(when))
         def _():
             act()
 
-    def a3():
-        x_wait(y, near[2], p)
-        view = slot(xg, y, near[2], p)
-        remote(view, view, xy_send.at[2], x_recv.at[y, near[2], p], ypeer).start()
-        x_to_partner(2, y, near[2]).start()
-
-    def b_next(i):
-        x_wait(1 - y, near[i], p)
-        x_to_partner(4 + i, 1 - y, near[i]).start()
+    def a_next(i):
+        x_wait(y, near[i], p)
+        view = slot(xg, y, near[i], p)
+        remote(view, view, xy_send.at[i], x_recv.at[y, near[i], p], ypeer).start()
+        x_to_partner(i, y, near[i]).start()
+
+    def b_next(i, c):
+        x_wait(1 - y, c, p)
+        x_to_partner(4 + i, 1 - y, c).start()
 
     def relay2():
         w_relay(2).start()
@@ -511,51 +522,15 @@
             b_wait(b, (fx, fy)[b])
             b_relay(b).start()
 
-    def body(k, carry):
-        event(k, 0, lambda: w_ready(0))
-        event(k, 2, a3)
-        event(k, 4, lambda: w_ready(1))
-        event(k, 4, relay2)
-        event(k, 5, lambda: b_next(0))
-        event(k, 7, lambda: w_relay(3).start())
-        event(k, 8, lambda: w_ready(2))
-        event(k, 9, lambda: b_next(1))
-        event(k, 10, lambda: b_next(2))
-        event(k, 10, back_own)
-        event(k, 12, lambda: w_ready(3))
-        event(k, 18, back_relay)
-
-        je = k - LAG_E * hop_e
-
-        @pl.when((je >= 0) & (je < steps))
-        def _():
-            step(0, je // nz, je % nz)
-
-        jl = k - LAG_L * hop_l - LATE
-
-        @pl.when((jl >= 0) & (jl < steps))
-        def _():
-            step(1, listed(LATE_MATS, jl), listed(LATE_CHUNKS, jl))
-
-        return carry
-
-    lax.fori_loop(0, steps + LATE + LAG_L * (nz - 1), body, 0)
-
-    owner = hop_e == nz - 1
-    is_end = (z == 0) | (z == nz - 1)
-    hop = hop_l
-    onward = toward_l
-
     def chain(b, q, c):
         view = yg.at[b, q, c]
         return remote(view, view, c_send.at[b, q, c], y_recv.at[b, q, c], onward)
 
-    @pl.when(is_end)
-    def _():
+    def heads(e):
+        s = y if e == 0 else 1 - y
         for k in range(nz):
-            view = start.at[piece(k, rs)]
-            remote(view, view, s_send.at[0], s_recv.at[k], partner).wait_recv()
-        e = hop_l // (nz - 1)
+            view = start.at[s, piece(k, rs)]
+            remote(view, view, s_send.at[0], s_recv.at[s, k], partner).wait_recv()
         small = group // 2
 
         def value_at(m, c):
@@ -582,7 +557,7 @@
             a, b = q_c[:, :small], q_c[:, small:]
             rq = jnp.concatenate([a * cosine - b * sine, a * sine + b * cosine], axis=-1)
             fade = jnp.exp(-((place + c * span).astype(f32) + 1.0) * r)
-            acc = jnp.dot((rq * fade).astype(bf), start[...], preferred_element_type=f32)
+            acc = jnp.dot((rq * fade).astype(bf), start[s], preferred_element_type=f32)
             rq = rq.astype(bf)
             for g in range(c + 1):
                 scores = lax.dot_general(
@@ -597,24 +572,55 @@
             differ = (trail / counts - value_at(3, c).astype(f32)).astype(bf)
             pooled = (jnp.dot(differ, mapv[...], preferred_element_type=f32) * scv[...]).astype(bf)
 
-            @pl.when(owner)
-            def _():
+            if e == 0:
                 yg[1, y, c] = ret
                 yg[0, y, c] = pooled
-                chain(1, y, c).start()
-                chain(0, y, c).start()
-
-            @pl.when(jnp.logical_not(owner))
-            def _():
+                for b in (1, 0):
+                    chain(b, y, c).start()
+            else:
                 yb[1, c] = ret
                 yb[0, c] = pooled
                 for b in (1, 0):
                     remote(yb.at[b, c], yg.at[b, y, c], h_send.at[b, c], y_recv.at[b, y, c], ypeer).start()
 
-    for b in range(2):
-        own_b[b].wait()
-        b_wait(b, (fy, fx)[b])
-        b_wait(b, fd)
+    def early_heads():
+        @pl.when(hop == nz - 1)
+        def _():
+            heads(0)
+
+    done_early = 1 + max(n for n, entry in enumerate(STEPS) if entry[0] == 0)
+    events = (
+        (places(0.0, lambda h, e, m, i: m == 0), lambda: w_ready(0)),
+        (places(10.5, lambda h, e, m, i: e == 1 and i == h), lambda: b_next(3, z)),
+        (places(12.5, lambda h, e, m, i: e == 0 and i == NEAR[h][1]), lambda: a_next(1)),
+        (places(13.2, lambda h, e, m, i: e == 0 and i == NEAR[h][2]), lambda: a_next(2)),
+        (places(13.3, lambda h, e, m, i: m == 2), relay2),
+        (places(13.5, lambda h, e, m, i: m == 1), lambda: w_ready(1)),
+        (places(16.4, lambda h, e, m, i: e == 1 and i == NEAR[h][0]), lambda: b_next(0, near[0])),
+        (places(18.5, lambda h, e, m, i: m == 3), lambda: w_relay(3).start()),
+        (places(20.0, lambda h, e, m, i: m == 2), lambda: w_ready(2)),
+        (places(22.0, lambda h, e, m, i: e == 1 and i == NEAR[h][1]), lambda: b_next(1, near[1])),
+        (places(24.8, lambda h, e, m, i: e == 1 and i == NEAR[h][2]), lambda: b_next(2, near[2])),
+        (places(25.2, lambda h, e, m, i: False), back_own),
+        (places(25.5, lambda h, e, m, i: m == 3), lambda: w_ready(3)),
+        ((done_early,) * 4, early_heads),
+        (places(36.5, lambda h, e, m, i: False), back_relay),
+    )
+
+    def body(n, carry):
+        for when, act in events:
+            event(n, when, act)
+        step(n)
+        return carry
+
+    lax.fori_loop(0, 2 * steps, body, 0)
+    event(2 * steps, *events[-1])
+
+    @pl.when(hop == nz - 1)
+    def _():
+        heads(1)
+
+    far = nz - 1 - hop
 
     def arrive(b, q, c):
         view = yg.at[b, q, c]
@@ -623,7 +629,7 @@
     def pass_on(b, q, c):
         arrive(b, q, c)
 
-        @pl.when(hop < nz - 1)
+        @pl.when(far < nz - 1)
         def _():
             chain(b, q, c).start()
 
@@ -636,7 +642,7 @@
         return acc
 
     def early(c):
-        @pl.when(hop > 0)
+        @pl.when(far > 0)
         def _():
             for b in (1, 0):
                 pass_on(b, y, c)
@@ -664,6 +670,11 @@
 
     for c in ORDER:
         early(c)
+    for b in range(2):
+        own_b[b].wait()
+        b_wait(b, (fy, fx)[b])
+        b_wait(b, fd)
+    for c in ORDER:
         keep[c] = product(y, c)
     for i, c in enumerate(ORDER):
         for b in (1, 0):
@@ -674,21 +685,21 @@
             then = i - late
             if late == 0 and then >= 0:
 
-                @pl.when(hop >= 2)
+                @pl.when(far >= 2)
                 def _():
                     finish(ORDER[then])
             if late == 2 and then >= 0:
 
-                @pl.when(hop == 1)
+                @pl.when(far == 1)
                 def _():
                     finish(ORDER[then])
 
-    @pl.when(hop == 1)
+    @pl.when(far == 1)
     def _():
         for c in ORDER[2:]:
             finish(c)
 
-    @pl.when(hop == 0)
+    @pl.when(far == 0)
     def _():
         for c in ORDER:
             finish(c)
@@ -701,23 +712,23 @@
         def _():
             remote(done.at[k], view, o_send.at[k], o_recv.at[k], partner).wait_send()
 
-    @pl.when(hop < nz - 1)
+    @pl.when(hop > 0)
     def _():
         for b in range(2):
             for q in range(2):
                 for c in range(nz):
                     chain(b, q, c).wait_send()
 
-    @pl.when(is_end & jnp.logical_not(owner))
+    @pl.when(hop == nz - 1)
     def _():
         for b in range(2):
             for c in range(nz):
                 remote(yb.at[b, c], yb.at[b, c], h_send.at[b, c], y_recv.at[b, 0, c], partner).wait_send()
 
-    for e in range(2):
-
-        @pl.when((hop_e if e == 0 else hop_l) < nz - 1)
-        def _():
+    @pl.when(hop < nz - 1)
+    def _():
+        for e in range(2):
+
             def drain(j, carry):
                 remote(obuf.at[e, j], rbuf.at[e, j], r_send.at[e, j], r_recv.at[e, j], partner).wait_send()
                 return carry
@@ -726,9 +737,9 @@
 
     for j in range(2):
 
-        @pl.when(jnp.logical_not((z == toward) & (y == j)))
-        def _():
-            remote(stb.at[j], stb.at[j], s_send.at[j], s_recv.at[0], partner).wait_send()
+        @pl.when(jnp.logical_not((z == goal) & (y == j)))
+        def _():
+            remote(stb.at[j], stb.at[j], s_send.at[j], s_recv.at[0, 0], partner).wait_send()
 
     for c in range(nz):
         give_copy(c).wait_send()
@@ -740,11 +751,12 @@
             b_own(b, i).wait_send()
         b_relay(b).wait_send()
     w_copy_x(3).wait_send()
-    for i in (2, 4, 5, 6):
+    for i in (1, 2, 4, 5, 6, 7):
         view = slot(xg, y, z, p)
         remote(view, view, xp_send.at[i], x_recv.at[y, z, p], partner).wait_send()
     view = slot(xg, y, z, p)
-    remote(view, view, xy_send.at[2], x_recv.at[y, z, p], partner).wait_send()
+    for i in (1, 2):
+        remote(view, view, xy_send.at[i], x_recv.at[y, z, p], partner).wait_send()
     for c in sent:
         c.wait_send()
 
@@ -791,7 +803,7 @@
             pltpu.VMEM((1, width), f32),
             pltpu.VMEM((2, rs, group), f32),
             pltpu.VMEM((2, rs, group), bf),
-            pltpu.VMEM((nsp * rs, group), bf),
+            pltpu.VMEM((2, nsp * rs, group), bf),
             pltpu.VMEM((length, group // 2), f32),
             pltpu.VMEM((length, group // 2), f32),
             pltpu.VMEM((group, group), bf),
@@ -807,7 +819,7 @@
             pltpu.VMEM((nsp, half, across), bf),
             dma((7,)), dma((4,)), dma((2,)), dma((4,)), dma((4,)), dma((4,)), dma((4, 4)),
             dma((3,)), dma((4,)), dma((8,)), dma((2, nsp, 2)),
-            dma((2,)), dma((nsp,)), dma((2, 3)), dma((2, 4)), dma((2, steps)), dma((2, steps)),
+            dma((2,)), dma((2, nsp)), dma((2, 3)), dma((2, 4)), dma((2, steps)), dma((2, steps)),
             dma((2, nsp)), dma((2, 2, nsp)), dma((2, 2, nsp)), dma((nsp,)), dma((nsp,)), dma((nsp,)), dma((nsp,)),
         ],
         compiler_params=pltpu.CompilerParams(collective_id=0, has_side_effects=True, vmem_limit_bytes=60 * 2**20),

time: 96.2 us -> 88.1 us (0.916)
  the two profiles are of different devices: /device:TPU:21 before, /device:TPU:17 now
where the time goes in v3:
time: 88.1 us; the launch traced here: 87.9 us
  Pallas kernels  86 us (98%)
  local copies, waits for them, and re-layouts  1.87 us (2%)
    pallas_call x1, Pallas kernels, paired(): pl.pallas_call(fused_kernel, out_shape=jax.ShapeDtypeStruct((half, width)...  86 us
    unnamed x1, local copies, waits for them, and re-layouts  1.87 us

profile of v3, /device:TPU:17, one launch (start us, length us, event | category | flops | bytes accessed | tf_op | source)
XLA Modules:
  0.0 87.9 jit_solution(3414907268388879534)
XLA Ops:
  0.0 86.0 %fused.1 = bf16[64,4096]{1,0:T(8,128)(2,1)} custom-call(bf16[128,4096]{1,0:T(8,128)(2,1)} %bitcast.6, f32[1,4096]{1,0:T(1,128)} %bitcast.8, bf16[256,512]{1,0:T(8,128)(2,1)} %wp.1, bf16[256,512]{1,0:T(8,128)(2,1)} %wq.1, bf16[256,512]{1,0:T(8,128)(2,1)} %wk.1, bf16[256,512]{1,0:T(8,128)(2,1)} %wv.1, f32[2,64,256]{2,1,0:T(8,128)} %bitcast.7, ...), custom_call_target="tpu_custom_call" | custom-call | tf_op jit(solution)/shard_map/fused/pallas_call | solution.py:790
  86.1 1.9 %copy.16 = bf16[1,64,4096]{2,1,0:T(8,128)(2,1)} copy(bf16[1,64,4096]{2,1,0:T(8,128)(2,1)} %bitcast.5) | data formatting | bytes 1048576

commit v4 on v3

--- a/solution.py
+++ b/solution.py
@@ -227,7 +227,7 @@
 
 
 MESH = pl.DeviceIdType.MESH
-ORDER = (0, 3, 1, 2)
+ORDER = (1, 2, 0, 3)
 STEPS = (
     (0, 0, 0, 10.0), (0, 0, 1, 10.7), (0, 1, 0, 14.0), (0, 1, 1, 14.7), (0, 0, 2, 15.4), (0, 1, 2, 16.1), (0, 0, 3, 16.8), (0, 1, 3, 17.5),
     (1, 0, 1, 18.2), (1, 1, 1, 18.9), (0, 2, 0, 20.3), (0, 2, 1, 21.0), (0, 2, 2, 21.7), (0, 2, 3, 22.4),
@@ -320,16 +320,6 @@
         c = pltpu.make_async_copy(mats[m].at[:, piece(y, group)], wg.at[m, piece(fs, rows)], wl_sem.at[m])
         c.start()
         own_w.append(c)
-    loads[0].wait()
-    loads[1].wait()
-
-    block = 16
-    for i in range(half // block):
-        floats = xt[i * block : (i + 1) * block, :].astype(f32)
-        xn[i * block : (i + 1) * block, :] = (
-            floats * lax.rsqrt(jnp.mean(floats * floats, axis=-1, keepdims=True) + eps) * gv[...]
-        ).astype(bf)
-
     def slot(ref, s, c, h):
         return ref.at[s, pl.ds(pl.multiple_of(c * span + h * half, half), half)]
 
@@ -371,6 +361,15 @@
 
     w_y(0)
     w_x(0)
+    loads[0].wait()
+    loads[1].wait()
+    block = 16
+    for i in range(half // block):
+        floats = xt[i * block : (i + 1) * block, :].astype(f32)
+        xn[i * block : (i + 1) * block, :] = (
+            floats * lax.rsqrt(jnp.mean(floats * floats, axis=-1, keepdims=True) + eps) * gv[...]
+        ).astype(bf)
+
     for i, c in enumerate(near):
         go(remote(xn.at[:, piece(c, feats)], slot(xg, y, z, p), xz_send.at[i], x_recv.at[y, z, p], at(c, y, x, p)))
     xg[y, pl.ds(pl.multiple_of(z * span + p * half, half), half), :] = xn[:, piece(z, feats)]
@@ -526,36 +525,35 @@
         view = yg.at[b, q, c]
         return remote(view, view, c_send.at[b, q, c], y_recv.at[b, q, c], onward)
 
-    def heads(e):
+    small = group // 2
+
+    def turned(values, c):
+        cosine, sine = cosv[c * span : (c + 1) * span, :], sinv[c * span : (c + 1) * span, :]
+        a, b = values[:, :small], values[:, small:]
+        return a * cosine - b * sine, a * sine + b * cosine
+
+    def hand_on(e, b, c, value):
+        if e == 0:
+            yg[b, y, c] = value
+            chain(b, y, c).start()
+        else:
+            yb[b, c] = value
+            remote(yb.at[b, c], yg.at[b, y, c], h_send.at[b, c], y_recv.at[b, y, c], ypeer).start()
+
+    place = lax.broadcasted_iota(jnp.int32, (span, 1), 0)
+
+    def retain(e):
         s = y if e == 0 else 1 - y
         for k in range(nz):
             view = start.at[s, piece(k, rs)]
             remote(view, view, s_send.at[0], s_recv.at[s, k], partner).wait_recv()
-        small = group // 2
-
-        def value_at(m, c):
-            return obuf[e, m * nz + c]
-
-        pool[0:HALO, :] = jnp.zeros((HALO, group), bf)
+        scale = group ** (-0.5)
         for c in range(nz):
-            cosine, sine = cosv[c * span : (c + 1) * span, :], sinv[c * span : (c + 1) * span, :]
-            k_c = value_at(0, c).astype(f32)
-            a, b = k_c[:, :small], k_c[:, small:]
-            scale = group ** (-0.5)
-            krot[c * span : (c + 1) * span, :small] = ((a * cosine - b * sine) * scale).astype(bf)
-            krot[c * span : (c + 1) * span, small:] = ((a * sine + b * cosine) * scale).astype(bf)
-            pool[HALO + c * span : HALO + (c + 1) * span, :] = value_at(3, c)
-        window = 2 * (1 + y) * (1 + 3 * p)
-        brow = lax.broadcasted_iota(jnp.int32, (span, span + HALO), 0)
-        bcol = lax.broadcasted_iota(jnp.int32, (span, span + HALO), 1)
-        behind = brow + HALO - bcol
-        band = jnp.where((behind >= 0) & (behind < window), 1.0, 0.0).astype(bf)
-        place = lax.broadcasted_iota(jnp.int32, (span, 1), 0)
+            first, second = turned(obuf[e, c].astype(f32), c)
+            krot[c * span : (c + 1) * span, :small] = (first * scale).astype(bf)
+            krot[c * span : (c + 1) * span, small:] = (second * scale).astype(bf)
         for c in ORDER:
-            cosine, sine = cosv[c * span : (c + 1) * span, :], sinv[c * span : (c + 1) * span, :]
-            q_c = value_at(1, c).astype(f32)
-            a, b = q_c[:, :small], q_c[:, small:]
-            rq = jnp.concatenate([a * cosine - b * sine, a * sine + b * cosine], axis=-1)
+            rq = jnp.concatenate(turned(obuf[e, nz + c].astype(f32), c), axis=-1)
             fade = jnp.exp(-((place + c * span).astype(f32) + 1.0) * r)
             acc = jnp.dot((rq * fade).astype(bf), start[s], preferred_element_type=f32)
             rq = rq.astype(bf)
@@ -564,30 +562,38 @@
                     rq, krot[g * span : (g + 1) * span, :], (((1,), (1,)), ((), ())), preferred_element_type=f32
                 )
                 scores = (scores * mask[c - g]).astype(bf)
-                acc += jnp.dot(scores, value_at(2, g), preferred_element_type=f32)
-            ret = (acc * lax.rsqrt(jnp.mean(acc * acc, axis=-1, keepdims=True) + eps)).astype(bf)
-            rows_c = pool[c * span : (c + 1) * span + HALO, :]
-            trail = jnp.dot(band, rows_c, preferred_element_type=f32)
+                acc += jnp.dot(scores, obuf[e, 2 * nz + g], preferred_element_type=f32)
+            hand_on(e, 1, c, (acc * lax.rsqrt(jnp.mean(acc * acc, axis=-1, keepdims=True) + eps)).astype(bf))
+
+    def gather_windows(e):
+        pool[0:HALO, :] = jnp.zeros((HALO, group), bf)
+        for c in range(nz):
+            pool[HALO + c * span : HALO + (c + 1) * span, :] = obuf[e, 3 * nz + c]
+        window = 2 * (1 + y) * (1 + 3 * p)
+        behind = (
+            lax.broadcasted_iota(jnp.int32, (span, span + HALO), 0) + HALO
+            - lax.broadcasted_iota(jnp.int32, (span, span + HALO), 1)
+        )
+        band = jnp.where((behind >= 0) & (behind < window), 1.0, 0.0).astype(bf)
+        for c in ORDER:
+            trail = jnp.dot(band, pool[c * span : (c + 1) * span + HALO, :], preferred_element_type=f32)
             counts = jnp.minimum(window, place + c * span + 1).astype(f32)
-            differ = (trail / counts - value_at(3, c).astype(f32)).astype(bf)
+            differ = (trail / counts - obuf[e, 3 * nz + c].astype(f32)).astype(bf)
             pooled = (jnp.dot(differ, mapv[...], preferred_element_type=f32) * scv[...]).astype(bf)
-
-            if e == 0:
-                yg[1, y, c] = ret
-                yg[0, y, c] = pooled
-                for b in (1, 0):
-                    chain(b, y, c).start()
-            else:
-                yb[1, c] = ret
-                yb[0, c] = pooled
-                for b in (1, 0):
-                    remote(yb.at[b, c], yg.at[b, y, c], h_send.at[b, c], y_recv.at[b, y, c], ypeer).start()
+            hand_on(e, 0, c, pooled)
 
     def early_heads():
         @pl.when(hop == nz - 1)
         def _():
-            heads(0)
-
+            retain(0)
+            gather_windows(0)
+
+    def late_heads():
+        @pl.when(hop == nz - 1)
+        def _():
+            retain(1)
+
+    done_late = 1 + max(n for n, entry in enumerate(STEPS) if entry[0] == 1 and entry[1] < 3)
     done_early = 1 + max(n for n, entry in enumerate(STEPS) if entry[0] == 0)
     events = (
         (places(0.0, lambda h, e, m, i: m == 0), lambda: w_ready(0)),
@@ -604,6 +610,7 @@
         (places(25.2, lambda h, e, m, i: False), back_own),
         (places(25.5, lambda h, e, m, i: m == 3), lambda: w_ready(3)),
         ((done_early,) * 4, early_heads),
+        ((done_late,) * 4, late_heads),
         (places(36.5, lambda h, e, m, i: False), back_relay),
     )
 
@@ -618,7 +625,7 @@
 
     @pl.when(hop == nz - 1)
     def _():
-        heads(1)
+        gather_windows(1)
 
     far = nz - 1 - hop
 
@@ -681,25 +688,11 @@
             pass_on(b, 1 - y, c)
         multiply(c)
 
-        for late in range(3):
-            then = i - late
-            if late == 0 and then >= 0:
-
-                @pl.when(far >= 2)
-                def _():
-                    finish(ORDER[then])
-            if late == 2 and then >= 0:
-
-                @pl.when(far == 1)
-                def _():
-                    finish(ORDER[then])
-
-    @pl.when(far == 1)
-    def _():
-        for c in ORDER[2:]:
+        @pl.when(far >= 2)
+        def _():
             finish(c)
 
-    @pl.when(far == 0)
+    @pl.when(far < 2)
     def _():
         for c in ORDER:
             finish(c)

time: 88.1 us -> 84.8 us (0.963)
  the two profiles are of different devices: /device:TPU:17 before, /device:TPU:29 now
where the time goes in v4:
time: 84.8 us; the launch traced here: 84.6 us
  Pallas kernels  82.8 us (98%)
  local copies, waits for them, and re-layouts  1.87 us (2%)
    pallas_call x1, Pallas kernels, paired(): pl.pallas_call(fused_kernel, out_shape=jax.ShapeDtypeStruct((half, width)...  82.8 us
    unnamed x1, local copies, waits for them, and re-layouts  1.87 us

profile of v4, /device:TPU:29, one launch (start us, length us, event | category | flops | bytes accessed | tf_op | source)
XLA Modules:
  0.0 84.6 jit_solution(1288474231503954635)
XLA Ops:
  0.0 82.8 %fused.1 = bf16[64,4096]{1,0:T(8,128)(2,1)} custom-call(bf16[128,4096]{1,0:T(8,128)(2,1)} %bitcast.6, f32[1,4096]{1,0:T(1,128)} %bitcast.8, bf16[256,512]{1,0:T(8,128)(2,1)} %wp.1, bf16[256,512]{1,0:T(8,128)(2,1)} %wq.1, bf16[256,512]{1,0:T(8,128)(2,1)} %wk.1, bf16[256,512]{1,0:T(8,128)(2,1)} %wv.1, f32[2,64,256]{2,1,0:T(8,128)} %bitcast.7, ...), custom_call_target="tpu_custom_call" | custom-call | tf_op jit(solution)/shard_map/fused/pallas_call | solution.py:783
  82.8 1.9 %copy.16 = bf16[1,64,4096]{2,1,0:T(8,128)(2,1)} copy(bf16[1,64,4096]{2,1,0:T(8,128)(2,1)} %bitcast.5) | data formatting | bytes 1048576

commit v5 on v4

--- a/solution.py
+++ b/solution.py
@@ -542,7 +542,7 @@
 
     place = lax.broadcasted_iota(jnp.int32, (span, 1), 0)
 
-    def retain(e):
+    def turn_keys(e):
         s = y if e == 0 else 1 - y
         for k in range(nz):
             view = start.at[s, piece(k, rs)]
@@ -552,6 +552,18 @@
             first, second = turned(obuf[e, c].astype(f32), c)
             krot[c * span : (c + 1) * span, :small] = (first * scale).astype(bf)
             krot[c * span : (c + 1) * span, small:] = (second * scale).astype(bf)
+
+    def heads(e):
+        s = y if e == 0 else 1 - y
+        pool[0:HALO, :] = jnp.zeros((HALO, group), bf)
+        for c in range(nz):
+            pool[HALO + c * span : HALO + (c + 1) * span, :] = obuf[e, 3 * nz + c]
+        window = 2 * (1 + y) * (1 + 3 * p)
+        behind = (
+            lax.broadcasted_iota(jnp.int32, (span, span + HALO), 0) + HALO
+            - lax.broadcasted_iota(jnp.int32, (span, span + HALO), 1)
+        )
+        band = jnp.where((behind >= 0) & (behind < window), 1.0, 0.0).astype(bf)
         for c in ORDER:
             rq = jnp.concatenate(turned(obuf[e, nz + c].astype(f32), c), axis=-1)
             fade = jnp.exp(-((place + c * span).astype(f32) + 1.0) * r)
@@ -564,18 +576,6 @@
                 scores = (scores * mask[c - g]).astype(bf)
                 acc += jnp.dot(scores, obuf[e, 2 * nz + g], preferred_element_type=f32)
             hand_on(e, 1, c, (acc * lax.rsqrt(jnp.mean(acc * acc, axis=-1, keepdims=True) + eps)).astype(bf))
-
-    def gather_windows(e):
-        pool[0:HALO, :] = jnp.zeros((HALO, group), bf)
-        for c in range(nz):
-            pool[HALO + c * span : HALO + (c + 1) * span, :] = obuf[e, 3 * nz + c]
-        window = 2 * (1 + y) * (1 + 3 * p)
-        behind = (
-            lax.broadcasted_iota(jnp.int32, (span, span + HALO), 0) + HALO
-            - lax.broadcasted_iota(jnp.int32, (span, span + HALO), 1)
-        )
-        band = jnp.where((behind >= 0) & (behind < window), 1.0, 0.0).astype(bf)
-        for c in ORDER:
             trail = jnp.dot(band, pool[c * span : (c + 1) * span + HALO, :], preferred_element_type=f32)
             counts = jnp.minimum(window, place + c * span + 1).astype(f32)
             differ = (trail / counts - obuf[e, 3 * nz + c].astype(f32)).astype(bf)
@@ -585,13 +585,13 @@
     def early_heads():
         @pl.when(hop == nz - 1)
         def _():
-            retain(0)
-            gather_windows(0)
+            turn_keys(0)
+            heads(0)
 
     def late_heads():
         @pl.when(hop == nz - 1)
         def _():
-            retain(1)
+            turn_keys(1)
 
     done_late = 1 + max(n for n, entry in enumerate(STEPS) if entry[0] == 1 and entry[1] < 3)
     done_early = 1 + max(n for n, entry in enumerate(STEPS) if entry[0] == 0)
@@ -625,7 +625,7 @@
 
     @pl.when(hop == nz - 1)
     def _():
-        gather_windows(1)
+        heads(1)
 
     far = nz - 1 - hop
 

time: 84.8 us -> 83.7 us (0.987); the launches traced: 84.6 us -> 82.5 us
  Pallas kernels: 82.8 us -> 80.6 us
    pallas_call x1, Pallas kernels: 82.8 us -> 80.6 us  [paired(): pl.pallas_call(fused_kernel, out_shape=jax.ShapeDtypeStruct((half, width)...]
where the time goes in v5:
time: 83.7 us; the launch traced here: 82.5 us
  Pallas kernels  80.6 us (96%)
  local copies, waits for them, and re-layouts  1.87 us (2%)
    pallas_call x1, Pallas kernels, paired(): pl.pallas_call(fused_kernel, out_shape=jax.ShapeDtypeStruct((half, width)...  80.6 us
    unnamed x1, local copies, waits for them, and re-layouts  1.87 us

profile of v5, /device:TPU:29, one launch (start us, length us, event | category | flops | bytes accessed | tf_op | source)
XLA Modules:
  0.0 82.5 jit_solution(9379886453536390660)
XLA Ops:
  0.0 80.6 %fused.1 = bf16[64,4096]{1,0:T(8,128)(2,1)} custom-call(bf16[128,4096]{1,0:T(8,128)(2,1)} %bitcast.6, f32[1,4096]{1,0:T(1,128)} %bitcast.8, bf16[256,512]{1,0:T(8,128)(2,1)} %wp.1, bf16[256,512]{1,0:T(8,128)(2,1)} %wq.1, bf16[256,512]{1,0:T(8,128)(2,1)} %wk.1, bf16[256,512]{1,0:T(8,128)(2,1)} %wv.1, f32[2,64,256]{2,1,0:T(8,128)} %bitcast.7, ...), custom_call_target="tpu_custom_call" | custom-call | tf_op jit(solution)/shard_map/fused/pallas_call | solution.py:783
  80.6 1.9 %copy.16 = bf16[1,64,4096]{2,1,0:T(8,128)(2,1)} copy(bf16[1,64,4096]{2,1,0:T(8,128)(2,1)} %bitcast.5) | data formatting | bytes 1048576

commit v6 on v5

--- a/solution.py
+++ b/solution.py
@@ -575,11 +575,12 @@
                 )
                 scores = (scores * mask[c - g]).astype(bf)
                 acc += jnp.dot(scores, obuf[e, 2 * nz + g], preferred_element_type=f32)
-            hand_on(e, 1, c, (acc * lax.rsqrt(jnp.mean(acc * acc, axis=-1, keepdims=True) + eps)).astype(bf))
+            ret = (acc * lax.rsqrt(jnp.mean(acc * acc, axis=-1, keepdims=True) + eps)).astype(bf)
             trail = jnp.dot(band, pool[c * span : (c + 1) * span + HALO, :], preferred_element_type=f32)
             counts = jnp.minimum(window, place + c * span + 1).astype(f32)
             differ = (trail / counts - obuf[e, 3 * nz + c].astype(f32)).astype(bf)
             pooled = (jnp.dot(differ, mapv[...], preferred_element_type=f32) * scv[...]).astype(bf)
+            hand_on(e, 1, c, ret)
             hand_on(e, 0, c, pooled)
 
     def early_heads():
@@ -598,9 +599,9 @@
     events = (
         (places(0.0, lambda h, e, m, i: m == 0), lambda: w_ready(0)),
         (places(10.5, lambda h, e, m, i: e == 1 and i == h), lambda: b_next(3, z)),
-        (places(12.5, lambda h, e, m, i: e == 0 and i == NEAR[h][1]), lambda: a_next(1)),
-        (places(13.2, lambda h, e, m, i: e == 0 and i == NEAR[h][2]), lambda: a_next(2)),
-        (places(13.3, lambda h, e, m, i: m == 2), relay2),
+        ((4, 1, 0, 0), lambda: a_next(1)),
+        ((4, 1, 0, 0), lambda: a_next(2)),
+        ((4, 2, 0, 0), relay2),
         (places(13.5, lambda h, e, m, i: m == 1), lambda: w_ready(1)),
         (places(16.4, lambda h, e, m, i: e == 1 and i == NEAR[h][0]), lambda: b_next(0, near[0])),
         (places(18.5, lambda h, e, m, i: m == 3), lambda: w_relay(3).start()),
@@ -784,7 +785,7 @@
         fused_kernel,
         out_shape=jax.ShapeDtypeStruct((half, width), bf),
         in_specs=[hbm] * 11 + [pl.BlockSpec(memory_space=pltpu.SMEM)] + [hbm] * 2,
-        out_specs=vm,
+        out_specs=hbm,
         scratch_shapes=[
             pltpu.VMEM((half, width), bf),
             pltpu.VMEM((half, width), bf),

time: 83.7 us -> 83.3 us (level); the launches traced: 82.5 us -> 83.1 us
  no operation moved by 1% of the time
where the time goes in v6:
time: 83.3 us; the launch traced here: 83.1 us
  Pallas kernels  81.3 us (98%)
  local copies, waits for them, and re-layouts  1.87 us (2%)
    pallas_call x1, Pallas kernels, paired(): pl.pallas_call(fused_kernel, out_shape=jax.ShapeDtypeStruct((half, width)...  81.3 us
    unnamed x1, local copies, waits for them, and re-layouts  1.87 us

profile of v6, /device:TPU:29, one launch (start us, length us, event | category | flops | bytes accessed | tf_op | source)
XLA Modules:
  0.0 83.1 jit_solution(656385341215834209)
XLA Ops:
  0.0 81.3 %fused.1 = bf16[64,4096]{1,0:T(8,128)(2,1)} custom-call(bf16[128,4096]{1,0:T(8,128)(2,1)} %bitcast.6, f32[1,4096]{1,0:T(1,128)} %bitcast.8, bf16[256,512]{1,0:T(8,128)(2,1)} %wp.1, bf16[256,512]{1,0:T(8,128)(2,1)} %wq.1, bf16[256,512]{1,0:T(8,128)(2,1)} %wk.1, bf16[256,512]{1,0:T(8,128)(2,1)} %wv.1, f32[2,64,256]{2,1,0:T(8,128)} %bitcast.7, ...), custom_call_target="tpu_custom_call" | custom-call | tf_op jit(solution)/shard_map/fused/pallas_call | solution.py:784
  81.3 1.9 %copy.16 = bf16[1,64,4096]{2,1,0:T(8,128)(2,1)} copy(bf16[1,64,4096]{2,1,0:T(8,128)(2,1)} %bitcast.5) | data formatting | bytes 1048576

commit v7 on v6

--- a/solution.py
+++ b/solution.py
@@ -396,17 +396,6 @@
     for j in range(2):
         stb[j] = st[j].astype(bf)
     rs = st.shape[1]
-    for j in range(2):
-        same = (z == goal) & (y == j)
-        dst = start.at[y, piece(z, rs)]
-
-        @pl.when(same)
-        def _():
-            pltpu.make_async_copy(stb.at[j], dst, s_recv.at[y, z]).start()
-
-        @pl.when(jnp.logical_not(same))
-        def _():
-            remote(stb.at[j], dst, s_send.at[j], s_recv.at[y, z], at(goal, j, x, p)).start()
 
     r = rate[y]
     row = lax.broadcasted_iota(jnp.int32, (span, span), 0)
@@ -506,6 +495,19 @@
     def b_next(i, c):
         x_wait(1 - y, c, p)
         x_to_partner(4 + i, 1 - y, c).start()
+
+    def state_out():
+        for j in range(2):
+            same = (z == goal) & (y == j)
+            dst = start.at[y, piece(z, rs)]
+
+            @pl.when(same)
+            def _():
+                pltpu.make_async_copy(stb.at[j], dst, s_recv.at[y, z]).start()
+
+            @pl.when(jnp.logical_not(same))
+            def _():
+                remote(stb.at[j], dst, s_send.at[j], s_recv.at[y, z], at(goal, j, x, p)).start()
 
     def relay2():
         w_relay(2).start()
@@ -602,6 +604,7 @@
         ((4, 1, 0, 0), lambda: a_next(1)),
         ((4, 1, 0, 0), lambda: a_next(2)),
         ((4, 2, 0, 0), relay2),
+        ((5, 2, 0, 0), state_out),
         (places(13.5, lambda h, e, m, i: m == 1), lambda: w_ready(1)),
         (places(16.4, lambda h, e, m, i: e == 1 and i == NEAR[h][0]), lambda: b_next(0, near[0])),
         (places(18.5, lambda h, e, m, i: m == 3), lambda: w_relay(3).start()),

time: 83.3 us -> 83.9 us (level)
  no operation moved by 1% of the time
where the time goes in v7:
time: 83.9 us; the launch traced here: 83.8 us
  Pallas kernels  81.9 us (98%)
  local copies, waits for them, and re-layouts  1.87 us (2%)
    pallas_call x1, Pallas kernels, paired(): pl.pallas_call(fused_kernel, out_shape=jax.ShapeDtypeStruct((half, width)...  81.9 us
    unnamed x1, local copies, waits for them, and re-layouts  1.87 us

profile of v7, /device:TPU:29, one launch (start us, length us, event | category | flops | bytes accessed | tf_op | source)
XLA Modules:
  0.0 83.8 jit_solution(15640056314335227544)
XLA Ops:
  0.0 81.9 %fused.1 = bf16[64,4096]{1,0:T(8,128)(2,1)} custom-call(bf16[128,4096]{1,0:T(8,128)(2,1)} %bitcast.6, f32[1,4096]{1,0:T(1,128)} %bitcast.8, bf16[256,512]{1,0:T(8,128)(2,1)} %wp.1, bf16[256,512]{1,0:T(8,128)(2,1)} %wq.1, bf16[256,512]{1,0:T(8,128)(2,1)} %wk.1, bf16[256,512]{1,0:T(8,128)(2,1)} %wv.1, f32[2,64,256]{2,1,0:T(8,128)} %bitcast.7, ...), custom_call_target="tpu_custom_call" | custom-call | tf_op jit(solution)/shard_map/fused/pallas_call | solution.py:787
  81.9 1.9 %copy.16 = bf16[1,64,4096]{2,1,0:T(8,128)(2,1)} copy(bf16[1,64,4096]{2,1,0:T(8,128)(2,1)} %bitcast.5) | data formatting | bytes 1048576
